TPU v7x, 256 devices: a whole 4x4x8 slice. The times are simulated.
256 devices in a mesh: rep: 32 (over z, y), fs: 4 (over x), tp: 2 (over core).
Axes of the slice: x: 4, y: 4, z: 8, core: 2. Of those that a mesh axis runs over, the one named last changes fastest.
Arguments:
- tokens: bfloat16 [32768, 2048], P(('rep', 'fs', 'tp')), may hold values from -24 to 24
- cotangent: bfloat16 [32768, 2048], P(('rep', 'fs', 'tp')), may hold values from -24 to 24
- gate_weight: bfloat16 [2048, 3072], P(None, 'fs'), may hold values from -0.125 to 0.125
- up_weight: bfloat16 [2048, 3072], P(None, 'fs'), may hold values from -0.125 to 0.125
- down_weight_t: bfloat16 [2048, 3072], P(None, 'fs'), may hold values from -0.109375 to 0.109375
Outputs:
- input_grad: bfloat16 [32768, 2048], P(('rep', 'fs', 'tp'))
- gate_grad: float32 [2048, 3072], P(('rep', 'tp'), 'fs')
- up_grad: float32 [2048, 3072], P(('rep', 'tp'), 'fs')
- down_grad: float32 [2048, 3072], P(('rep', 'tp'), 'fs')
All inputs are finite; a program needn't handle non-finite values.
Results may differ from a plain program's by a relative error of at most 0.012.
Values may be sent and summed in bfloat16 or wider, within the bound.
A program may use at most 128 MiB of HBM per device.

v0:
```python
import jax
import jax.numpy as jnp
from jax import lax
from jax.sharding import PartitionSpec as P


def joined_along(parts, dim):
    parts = jnp.moveaxis(parts, 0, dim)
    shape = parts.shape
    return parts.reshape(*shape[:dim], shape[dim] * shape[dim + 1], *shape[dim + 2 :])


def copy_for_each(value, axis):
    copies = jnp.broadcast_to(value, (lax.axis_size(axis), *value.shape))
    return lax.all_to_all(copies, axis, split_axis=0, concat_axis=0, tiled=True)


def gathered_copies(value, axis, dim):
    return joined_along(copy_for_each(value, axis), dim)


def in_one_piece(arrays, axis, dim, along):
    widths = [a.shape[along] for a in arrays]
    both = jnp.concatenate(arrays, axis=along)
    whole = gathered_copies(both, axis, dim)
    return tuple(jnp.split(whole, [sum(widths[:k]) for k in range(1, len(widths))], axis=along))


def in_blocks(value, dim, peers):
    before, after = (value.shape[:dim], value.shape[dim + 1 :])
    return jnp.moveaxis(value.reshape(*before, peers, -1, *after), dim, 0)


def sum_at_owner(value, axis, dim):
    parts = in_blocks(value, dim, lax.axis_size(axis))
    arrived = lax.all_to_all(parts, axis, split_axis=0, concat_axis=0, tiled=True)
    return arrived.astype(jnp.float32).sum(axis=0)


def in_one_piece_2(arrays, axis, dim, along):
    both = jnp.concatenate(arrays, axis=along)
    whole, at, finished = (lax.psum_scatter(both, axis, scatter_dimension=dim, tiled=True), 0, [])
    for a in arrays:
        finished.append(lax.slice_in_dim(whole, at, at + a.shape[along], axis=along))
        at += a.shape[along]
    return tuple(finished)


def on_device(tokens, cotangent, gate_weight, up_weight, down_weight_t):
    tok_rows, cot_rows = in_one_piece((tokens, cotangent), "fs", 0, 1)
    gate_pre = jnp.dot(tok_rows, gate_weight, preferred_element_type=jnp.float32)
    up_pre = jnp.dot(tok_rows, up_weight, preferred_element_type=jnp.float32)
    sig_gate = jax.nn.sigmoid(gate_pre)
    act_gate = gate_pre * sig_gate
    hidden = (act_gate * up_pre).astype(jnp.bfloat16)
    hid_grad = jnp.dot(cot_rows, down_weight_t, preferred_element_type=jnp.float32)
    local_gate_back = (hid_grad * up_pre * sig_gate * (1.0 + gate_pre * (1.0 - sig_gate))).astype(
        jnp.bfloat16
    )
    local_up_back = (hid_grad * act_gate).astype(jnp.bfloat16)
    tok_all, cot_all, gate_back, up_back, hidden = (
        tok_rows,
        cot_rows,
        local_gate_back,
        local_up_back,
        hidden,
    )
    own_rows = tokens.shape[0]
    across = (((1,), (1,)), ((), ()))
    input_grad = sum_at_owner(
        (
            lax.dot_general(gate_back, gate_weight, across, preferred_element_type=jnp.float32)
            + lax.dot_general(up_back, up_weight, across, preferred_element_type=jnp.float32)
        ).astype(jnp.bfloat16),
        "fs",
        0,
    ).astype(jnp.bfloat16)
    replicas = lax.axis_size("rep")
    cores = lax.axis_size("tp")
    shards = lax.axis_size("fs")
    grad_scale = float(own_rows * replicas * shards * cores) ** (-0.5)
    down_rows = (((0,), (0,)), ((), ()))
    gate_local = (
        lax.dot_general(tok_all, gate_back, down_rows, preferred_element_type=jnp.float32)
        * grad_scale
    )
    up_local = (
        lax.dot_general(tok_all, up_back, down_rows, preferred_element_type=jnp.float32)
        * grad_scale
    )
    down_local = (
        lax.dot_general(cot_all, hidden, down_rows, preferred_element_type=jnp.float32) * grad_scale
    )
    summed = in_one_piece_2((gate_local, up_local, down_local), ("rep", "tp"), 0, 1)
    return (input_grad, summed[0], summed[1], summed[2])


def solution(mesh):
    return jax.shard_map(
        on_device,
        mesh=mesh,
        in_specs=(
            P(("rep", "fs", "tp"), None),
            P(("rep", "fs", "tp"), None),
            P(None, "fs"),
            P(None, "fs"),
            P(None, "fs"),
        ),
        out_specs=(
            P(("rep", "fs", "tp"), None),
            P(("rep", "tp"), "fs"),
            P(("rep", "tp"), "fs"),
            P(("rep", "tp"), "fs"),
        ),
        check_vma=False,
    )
```

profile of v0, /device:TPU:32, one launch (start us, length us, event | category | flops | bytes accessed | tf_op | source)
XLA Modules:
  0.0 305.6 jit_solution(6540316080608797469)
XLA Ops:
  7.2 0.0 copy-start
  7.2 0.0 reduce-scatter.4.cloned.1.call-start
  7.2 1.4 pad_maximum_fusion.1
  8.7 0.5 broadcast_in_dim.3
  9.2 52.9 %all_to_all.10 = bf16[4,128,4096]{2,1,0:T(8,128)(2,1)S(1)} all-to-all(bf16[4,128,4096]{2,1,0:T(8,128)(2,1)S(1)} %broadcast_in_dim.3), channel_id=1, replica_groups=mesh['rep'=32,'fs'=4,'tp'=2] {'fs'}, dimensions={0} | all-to-all | bytes 8388608 | tf_op jit(solution)/shard_map/all_to_all | solution.py:15
  62.1 0.0 copy-done
  62.1 1.8 fusion.6
  63.9 0.1 copy-done.5
  64.0 1.8 fusion.8
  65.8 0.0 copy-start.4
  65.8 2.0 convolution_multiply_fusion
  67.8 2.2 multiply_convert_fusion.1
  70.0 1.9 convolution_multiply_fusion.1
  71.9 1.9 convolution_multiply_fusion.2
  73.8 7.1 %pad_maximum_fusion = f32[2048,2304]{0,1:T(8,128)} fusion(f32[2048,768]{0,1:T(8,128)S(1)} %convolution_multiply_fusion, f32[2048,768]{0,1:T(8,128)S(1)} %convolution_multiply_fusion.1, f32[2048,768]{0,1:T(8,128)S(1)} %convolution_multiply_fusion.2), kind=kLoop, calls=%fused_computation | loop fusion | flops 9437184 | bytes 37748736 | tf_op jit(solution)/shard_map/concatenate | solution.py:41
  80.9 18.7 %copy.15 = f32[2048,2304]{1,0:T(8,128)} copy(f32[2048,2304]{0,1:T(8,128)} %pad_maximum_fusion) | data formatting | bytes 37748736
  99.6 0.0 reduce-scatter.4.cloned.1.call-update
  99.7 0.0 copy-start.6
  99.7 3.1 %fusion.13 = f32[512,2048]{1,0:T(8,128)S(1)} fusion(bf16[512,768]{1,0:T(8,128)(2,1)} %copy-done.3, bf16[2048,768]{1,0:T(8,128)(2,1)S(1)} %copy-done), kind=kOutput, calls=%fused_computation.22 | convolution fusion | flops 1610612736 | bytes 8126464 | tf_op jit(solution)/shard_map/dot_general | solution.py:72
  102.8 1.8 add_convert_fusion
  104.6 28.7 %all_to_all.11 = bf16[4,128,2048]{2,1,0:T(8,128)(2,1)} all-to-all(bf16[4,128,2048]{2,1,0:T(8,128)(2,1)S(1)} %bitcast.18), channel_id=1, replica_groups=mesh['rep'=32,'fs'=4,'tp'=2] {'fs'}, dimensions={0} | all-to-all | bytes 4194304 | tf_op jit(solution)/shard_map/all_to_all | solution.py:36
  133.3 3.0 reduce_sum.12
  136.4 160.7 %reduce-scatter.4.cloned.1.call-done = f32[32,2304]{1,0:T(8,128)} async-done(((f32[2048,2304]{1,0:T(8,128)}), f32[32,2304]{1,0:T(8,128)}) %reduce-scatter.4.cloned.1.call-update) | async-done | bytes 294928
  297.1 1.7 fusion.12
  (9 shorter events, 0.0 us)
Async XLA Ops:
  7.2 54.9 %copy-start = (bf16[2048,768]{1,0:T(8,128)(2,1)S(1)}, bf16[2048,768]{1,0:T(8,128)(2,1)}, u32[]{:S(2)}) copy-start(bf16[2048,768]{1,0:T(8,128)(2,1)} %param.7) | copy-start | bytes 9437188
  7.2 289.9 %reduce-scatter.4.cloned.1.call-start = ((), (), s32[]{:S(2)}) async-start(), calls=%async_computation.3 | async-start | bytes 19169280
  62.1 1.9 copy-start.5
  65.8 2.0 copy-start.4
  70.0 1.9 copy-start.1
  70.0 1.9 copy-start.3
  99.6 3.1 %copy-start.2 = (bf16[512,768]{1,0:T(8,128)(2,1)S(1)}, bf16[512,768]{1,0:T(8,128)(2,1)}, u32[]{:S(2)}) copy-start(bf16[512,768]{1,0:T(8,128)(2,1)} %copy-done.1) | copy-start | bytes 2359300
  99.7 3.1 %copy-start.6 = (bf16[2048,768]{1,0:T(8,128)(2,1)S(1)}, bf16[2048,768]{1,0:T(8,128)(2,1)}, u32[]{:S(2)}) copy-start(bf16[2048,768]{1,0:T(8,128)(2,1)} %param.8) | copy-start | bytes 9437188
Sparse Core Ops, SparseCore 0:
  99.8 197.2 reduce-scatter.3
where the time goes:
time: 307 us; the launch traced here: 306 us
  waiting for transfers between devices  161 us (52%)
  blocking collectives  81.6 us (27%)
  local copies, waits for them, and re-layouts  21 us (7%)
  matrix products  16.5 us (5%)
  between operations  14.2 us (5%)
  other arithmetic  11.6 us (4%)
    unnamed x2, waiting for transfers between devices  161 us
    all_to_all x1, blocking collectives, copy_for_each(): return lax.all_to_all(copies, axis, split_axis=0, concat_axis=0, tiled=True)  52.9 us
    all_to_all x1, blocking collectives, sum_at_owner(): lax.all_to_all(parts, axis, split_axis=0, concat_axis=0, tiled=True)  28.7 us
    unnamed x15, local copies, waits for them, and re-layouts  18.8 us
    concatenate x1, other arithmetic, in_one_piece_2(): both = jnp.concatenate(arrays, axis=along)  7.1 us
  transfers between devices with their start and end apart: 1, of which 1 were waited for; matrix products, arithmetic and copies ran while one was open for 3% of the time, Pallas kernels for 0%

commit v1 on v0

v1 whole, which is shorter than its diff:
```python
import functools

import jax
import jax.numpy as jnp
from jax import lax
from jax.experimental import pallas as pl
from jax.experimental.pallas import tpu as pltpu
from jax.sharding import PartitionSpec as P

MESH = pl.DeviceIdType.MESH
F32 = jnp.float32
BF16 = jnp.bfloat16
NY = 4


def body(
    nz, scale, tok_hbm, cot_hbm, gw_hbm, uw_hbm, dw_hbm, ig_ref, gg_ref, ug_ref, dg_ref,
    tok, cot, tokt, cott, gw, uw, dw, gpre, upre, hid, gb, ub, part, xhalf, xfull,
    prod, peer, summed, ya, za, zb, yb,
    ld_sem, ag_s, ag_r, dd_s, dd_r, xs_s, xs_r, rs_s, rs_r,
):
    rep = lax.axis_index("rep")
    x = lax.axis_index("fs")
    t = lax.axis_index("tp")
    nx = 4
    rows = tok.shape[1]
    half = rows // 2
    ff = gw.shape[1]
    d = gw.shape[0]
    z = rep // NY
    y = lax.rem(rep, NY)
    nxt, prv, opp = lax.rem(x + 1, nx), lax.rem(x + nx - 1, nx), lax.rem(x + 2, nx)
    other = 1 - t
    sgn = 1 - 2 * t

    def along_y(step):
        return lax.rem(y + NY + step, NY)

    def along_z(step):
        return lax.rem(z + nz + step, nz)

    def dev_y(step):
        return {"rep": z * NY + along_y(step)}

    def dev_z(step):
        return {"rep": along_z(step) * NY + y}

    loads = [
        pltpu.make_async_copy(src, dst, ld_sem.at[k])
        for k, (src, dst) in enumerate(
            [(tok_hbm, tok.at[x]), (gw_hbm, gw), (uw_hbm, uw), (cot_hbm, cot.at[x]), (dw_hbm, dw)]
        )
    ]
    for load in loads:
        load.start()

    barrier = pltpu.get_barrier_semaphore()
    peers = [{"fs": nxt}, {"fs": prv}, {"tp": other}, dev_y(1), dev_y(-1), dev_z(1), dev_z(-1)]
    for who in peers:
        pl.semaphore_signal(barrier, inc=1, device_id=who, device_id_type=MESH)
    pl.semaphore_wait(barrier, len(peers))

    def remote(src, dst, s, r, who):
        return pltpu.make_async_remote_copy(
            src_ref=src, dst_ref=dst, send_sem=s, recv_sem=r, device_id=who, device_id_type=MESH
        )

    bufs = (tok, cot)
    to = ({"fs": nxt}, {"fs": prv})
    came = (prv, nxt)

    def gather(a, way, k, slot, h):
        ref = bufs[a].at[slot, pl.ds(h * half, half), :]
        return remote(ref, ref, ag_s.at[a, way, k], ag_r.at[a, way, k], to[way])

    def gather_out(a):
        for k in range(2):
            for way in range(2):
                gather(a, way, k, x, k if way == 0 else 1 - k).start()

    def gather_in(a, way, k):
        if k == 2:
            gather(a, way, 2, opp, way).wait_recv()
        else:
            gather(a, way, k, came[way], k if way == 0 else 1 - k).wait_recv()

    def pass_on(a):
        for way in range(2):
            gather_in(a, way, 0)
            gather(a, way, 2, came[way], way).start()

    nt = 256

    def turned(src, dst, slot):
        at = pl.ds(pl.multiple_of(slot * rows, rows), rows)

        def one(i, _):
            cols = pl.ds(pl.multiple_of(i * nt, nt), nt)
            dst[cols, at] = src[slot, :, cols].T
            return 0

        lax.fori_loop(0, d // nt, one, 0)

    def forward(slot):
        def one(i, _):
            cols = pl.ds(pl.multiple_of(i * nt, nt), nt)
            g = jnp.dot(tok[slot], gw[:, cols], preferred_element_type=F32)
            u = jnp.dot(tok[slot], uw[:, cols], preferred_element_type=F32)
            gpre[slot, :, cols] = g
            upre[slot, :, cols] = u
            hid[slot, :, cols] = (g * jax.nn.sigmoid(g) * u).astype(BF16)
            return 0

        lax.fori_loop(0, ff // nt, one, 0)
        turned(tok, tokt, slot)

    def backward(slot):
        def one(i, _):
            cols = pl.ds(pl.multiple_of(i * nt, nt), nt)
            h = jnp.dot(cot[slot], dw[:, cols], preferred_element_type=F32)
            g = gpre[slot, :, cols]
            sig = jax.nn.sigmoid(g)
            gb[slot, :, cols] = (h * upre[slot, :, cols] * sig * (1.0 + g * (1.0 - sig))).astype(BF16)
            ub[slot, :, cols] = (h * (g * sig)).astype(BF16)
            return 0

        lax.fori_loop(0, ff // nt, one, 0)
        turned(cot, cott, slot)

    def input_part(slot):
        across = (((1,), (1,)), ((), ()))

        def one(i, _):
            cols = pl.ds(pl.multiple_of(i * nt, nt), nt)
            p = lax.dot_general(gb[slot], gw[cols, :], across, preferred_element_type=F32)
            p += lax.dot_general(ub[slot], uw[cols, :], across, preferred_element_type=F32)
            part[slot, :, cols] = p.astype(BF16)
            return 0

        lax.fori_loop(0, d // nt, one, 0)

    def x_first(way):
        return remote(
            part.at[opp, pl.ds(way * half, half), :], xhalf.at[way], xs_s.at[way], xs_r.at[way], to[way]
        )

    def x_second(way):
        return remote(part.at[(nxt, prv)[way]], xfull.at[way], xs_s.at[2 + way], xs_r.at[2 + way], to[way])

    def x_start():
        for way in range(2):
            x_first(way).start()

    def x_forward():
        for way in range(2):
            x_first(way).wait_recv()
            slot = (nxt, prv)[way]
            for i in range(half // 16):
                at = pl.ds(way * half + i * 16, 16)
                got = xhalf[way, pl.ds(i * 16, 16), :].astype(F32)
                part[slot, at, :] = (part[slot, at, :].astype(F32) + got).astype(BF16)
            x_second(way).start()

    def x_finish():
        for way in range(2):
            x_second(way).wait_recv()

        def one(i, _):
            at = pl.ds(pl.multiple_of(i * 16, 16), 16)
            total = part[x, at, :].astype(F32) + xfull[0, at, :].astype(F32) + xfull[1, at, :].astype(F32)
            ig_ref[at, :] = total.astype(BF16)
            return 0

        lax.fori_loop(0, rows // 16, one, 0)

    def pair(k, i):
        return remote(prod.at[k, i, :, other], peer.at[k, i], dd_s.at[k, i], dd_r.at[k, i], {"tp": other})

    dt = NY * 2 * 32

    def weight_sums(k, left, right):
        def one(i, _):
            lines = pl.ds(pl.multiple_of(i * dt, dt), dt)
            for j in range(ff // nt):
                cols = pl.ds(j * nt, nt)
                acc = jnp.dot(left[lines, 0:rows], right[0, :, cols], preferred_element_type=F32)
                for s in range(1, nx):
                    acc += jnp.dot(
                        left[lines, s * rows : (s + 1) * rows], right[s, :, cols], preferred_element_type=F32
                    )
                prod[k, i, :, :, :, cols] = acc.astype(BF16).reshape(NY, 2, 32, nt)
            pair(k, i).start()
            return 0

        lax.fori_loop(0, nz, one, 0)

    fa = ff // 2

    def pair_sum(k):
        def one(i, _):
            pair(k, i).wait_recv()
            for j in range(NY):
                both = prod[k, i, j, t].astype(F32) + peer[k, i, j].astype(F32)
                both = both.astype(BF16)
                summed[k, 0, i, j] = both[:, :fa]
                summed[k, 1, i, j] = both[:, fa:]
            return 0

        lax.fori_loop(0, nz, one, 0)

    ly, lz = (NY // 2, (NY - 1) // 2), (nz // 2, (nz - 1) // 2)
    per = sum(ly) + sum(lz)

    def chain_copy(k, half_no, axis, way, step):
        n_first = (ly, lz)[axis][0]
        m = step if way == 0 else n_first + step
        go = sgn if way == 0 else -sgn
        dist = ((ly, lz)[axis][way] - step) * go
        if half_no == 0:
            if axis == 0:
                src, dst = summed.at[k, 0, :, along_y(dist)], ya.at[k, m]
            else:
                src, dst = summed.at[k, 0, along_z(dist), y], za.at[k, m]
        else:
            if axis == 1:
                src, dst = summed.at[k, 1, along_z(dist)], zb.at[k, m]
            else:
                src, dst = summed.at[k, 1, z, along_y(dist)], yb.at[k, m]
        who = dev_y(go) if axis == 0 else dev_z(go)
        n = m if axis == (0 if half_no == 0 else 1) else (sum(ly) if half_no == 0 else sum(lz)) + m
        return remote(src, dst, rs_s.at[k, half_no, n], rs_r.at[k, half_no, n], who)

    def add_block(k, half_no, axis, step_to, ms):
        if half_no == 0 and axis == 0:
            at = along_y(step_to)

            def one(i, _):
                v = summed[k, 0, i, at].astype(F32)
                for m in ms:
                    v += ya[k, m, i].astype(F32)
                summed[k, 0, i, at] = v.astype(BF16)
                return 0

            lax.fori_loop(0, nz, one, 0)
        elif half_no == 0:
            at = along_z(step_to)
            v = summed[k, 0, at, y].astype(F32)
            for m in ms:
                v += za[k, m].astype(F32)
            summed[k, 0, at, y] = v.astype(BF16)
        elif axis == 1:
            at = along_z(step_to)

            def one(i, _):
                v = summed[k, 1, at, i].astype(F32)
                for m in ms:
                    v += zb[k, m, i].astype(F32)
                summed[k, 1, at, i] = v.astype(BF16)
                return 0

            lax.fori_loop(0, NY, one, 0)
        else:
            at = along_y(step_to)
            v = summed[k, 1, z, at].astype(F32)
            for m in ms:
                v += yb[k, m].astype(F32)
            summed[k, 1, z, at] = v.astype(BF16)

    outs = (dg_ref, gg_ref, ug_ref)

    def chain_step(k, half_no, axis, step):
        lens = (ly, lz)[axis]
        for way in range(2):
            if step >= lens[way]:
                continue
            if step > 0:
                chain_copy(k, half_no, axis, way, step - 1).wait_recv()
                go = sgn if way == 0 else -sgn
                m = step - 1 if way == 0 else lens[0] + step - 1
                add_block(k, half_no, axis, (lens[way] - step) * go, [m])
            chain_copy(k, half_no, axis, way, step).start()

    def chain_end(k, half_no, axis, last):
        lens = (ly, lz)[axis]
        ms = []
        for way in range(2):
            if lens[way]:
                chain_copy(k, half_no, axis, way, lens[way] - 1).wait_recv()
                ms.append(lens[way] - 1 if way == 0 else lens[0] + lens[1] - 1)
        if not last:
            add_block(k, half_no, axis, 0, ms)
            return
        v = summed[k, half_no, z, y].astype(F32)
        for m in ms:
            v += (za if half_no == 0 else yb)[k, m].astype(F32)
        outs[k][:, half_no * fa : (half_no + 1) * fa] = v * scale

    def stage(k, half_no, n):
        first, second = (0, 1) if half_no == 0 else (1, 0)
        n1, n2 = (ly, lz)[first][0], (ly, lz)[second][0]
        if n < n1:
            chain_step(k, half_no, first, n)
        elif n == n1:
            chain_end(k, half_no, first, False)
            chain_step(k, half_no, second, 0)
        elif n < n1 + n2:
            chain_step(k, half_no, second, n - n1)
        elif n == n1 + n2:
            chain_end(k, half_no, second, True)

    loads[0].wait()
    gather_out(0)
    loads[1].wait()
    loads[2].wait()
    forward(x)
    pass_on(0)
    loads[3].wait()
    gather_out(1)
    loads[4].wait()
    backward(x)
    input_part(x)
    gather_in(0, 0, 1)
    forward(prv)
    gather_in(0, 1, 1)
    forward(nxt)
    gather_in(0, 0, 2)
    gather_in(0, 1, 2)
    forward(opp)
    pass_on(1)
    gather_in(1, 0, 1)
    backward(prv)
    gather_in(1, 1, 1)
    backward(nxt)
    input_part(prv)
    input_part(nxt)
    gather_in(1, 0, 2)
    gather_in(1, 1, 2)
    backward(opp)
    weight_sums(0, cott, hid)
    weight_sums(1, tokt, gb)
    pair_sum(0)
    stage(0, 0, 0)
    stage(0, 1, 0)
    weight_sums(2, tokt, ub)
    pair_sum(1)
    stage(1, 0, 0)
    stage(1, 1, 0)
    input_part(opp)
    x_start()
    pair_sum(2)
    stage(2, 0, 0)
    stage(2, 1, 0)
    n_stages = ly[0] + lz[0] + 1
    for n in range(1, n_stages):
        for k in range(3):
            stage(k, 1, n)
            stage(k, 0, n)
        if n == 1:
            x_forward()
        if n == 4:
            x_finish()

    for a in range(2):
        for way in range(2):
            for k in range(2):
                gather(a, way, k, x, k if way == 0 else 1 - k).wait_send()
            gather(a, way, 2, came[way], way).wait_send()
    for way in range(2):
        x_first(way).wait_send()
        x_second(way).wait_send()

    def drain(i, _):
        for k in range(3):
            pair(k, i).wait_send()
        return 0

    lax.fori_loop(0, nz, drain, 0)
    for k in range(3):
        for half_no in range(2):
            for axis in range(2):
                for way in range(2):
                    for step in range((ly, lz)[axis][way]):
                        chain_copy(k, half_no, axis, way, step).wait_send()


def solution(mesh):
    n_rep = mesh.shape["rep"]
    nz = n_rep // NY
    nx = mesh.shape["fs"]
    cores = mesh.shape["tp"]

    def on_device(tokens, cotangent, gate_weight, up_weight, down_weight_t):
        rows, d = tokens.shape
        ff = gate_weight.shape[1]
        scale = float(rows * n_rep * nx * cores) ** (-0.5)
        lines = d // (n_rep * cores)
        fa = ff // 2
        ny_msgs, nz_msgs = NY - 1, nz - 1
        grad = jax.ShapeDtypeStruct((lines, ff), F32)
        vmem = pl.BlockSpec(memory_space=pltpu.VMEM)
        dma = pltpu.SemaphoreType.DMA
        return pl.pallas_call(
            functools.partial(body, nz, scale),
            out_shape=(jax.ShapeDtypeStruct((rows, d), BF16), grad, grad, grad),
            in_specs=[pl.BlockSpec(memory_space=pl.ANY)] * 5,
            out_specs=(vmem,) * 4,
            scratch_shapes=[
                pltpu.VMEM((nx, rows, d), BF16),
                pltpu.VMEM((nx, rows, d), BF16),
                pltpu.VMEM((d, nx * rows), BF16),
                pltpu.VMEM((d, nx * rows), BF16),
                pltpu.VMEM((d, ff), BF16),
                pltpu.VMEM((d, ff), BF16),
                pltpu.VMEM((d, ff), BF16),
                pltpu.VMEM((nx, rows, ff), F32),
                pltpu.VMEM((nx, rows, ff), F32),
                pltpu.VMEM((nx, rows, ff), BF16),
                pltpu.VMEM((nx, rows, ff), BF16),
                pltpu.VMEM((nx, rows, ff), BF16),
                pltpu.VMEM((nx, rows, d), BF16),
                pltpu.VMEM((2, rows // 2, d), BF16),
                pltpu.VMEM((2, rows, d), BF16),
                pltpu.VMEM((3, nz, NY, cores, lines, ff), BF16),
                pltpu.VMEM((3, nz, NY, lines, ff), BF16),
                pltpu.VMEM((3, 2, nz, NY, lines, fa), BF16),
                pltpu.VMEM((3, ny_msgs, nz, lines, fa), BF16),
                pltpu.VMEM((3, nz_msgs, lines, fa), BF16),
                pltpu.VMEM((3, nz_msgs, NY, lines, fa), BF16),
                pltpu.VMEM((3, ny_msgs, lines, fa), BF16),
                dma((5,)),
                dma((2, 2, 3)),
                dma((2, 2, 3)),
                dma((3, nz)),
                dma((3, nz)),
                dma((4,)),
                dma((4,)),
                dma((3, 2, ny_msgs + nz_msgs)),
                dma((3, 2, ny_msgs + nz_msgs)),
            ],
            compiler_params=pltpu.CompilerParams(
                collective_id=0, has_side_effects=True, vmem_limit_bytes=64 * 1024 * 1024 - 128 * 1024
            ),
        )(tokens, cotangent, gate_weight, up_weight, down_weight_t)

    return jax.shard_map(
        on_device,
        mesh=mesh,
        in_specs=(
            P(("rep", "fs", "tp"), None),
            P(("rep", "fs", "tp"), None),
            P(None, "fs"),
            P(None, "fs"),
            P(None, "fs"),
        ),
        out_specs=(
            P(("rep", "fs", "tp"), None),
            P(("rep", "tp"), "fs"),
            P(("rep", "tp"), "fs"),
            P(("rep", "tp"), "fs"),
        ),
        check_vma=False,
    )
```

time: 307 us -> 106 us (0.35)
  waiting for transfers between devices: 161 us -> 0 us
  Pallas kernels: 0 us -> 98.2 us
  blocking collectives: 81.6 us -> 0 us
  matrix products: 16.5 us -> 0 us
  local copies, waits for them, and re-layouts: 21 us -> 6.5 us
  between operations: 14.2 us -> 0.64 us
  other arithmetic: 11.6 us -> 0 us
    unnamed x2 -> x0, waiting for transfers between devices: 161 us -> none
    pallas_call x0 -> x1, Pallas kernels: none -> 98.2 us  [on_device(): pl.pallas_call(functools.partial(body, nz, scale), out_shape=(jax.ShapeDt...]
    all_to_all x2 -> x0, blocking collectives: 81.6 us -> none  [the longest x1 52.9 us: copy_for_each(): return lax.all_to_all(copies, axis, split_axis=0, concat_axis=0, tiled=True)]
    dot_general x8 -> x0, matrix products: 16.5 us -> none  [the longest x1 3.11 us: on_device(): lax.dot_general(gate_back, gate_weight, across, preferred_element_type=jn...]
    unnamed x15 -> x4, local copies, waits for them, and re-layouts: 18.8 us -> 6.5 us
    concatenate x2 -> x0, other arithmetic: 8.54 us -> none  [the longest x1 7.1 us: in_one_piece_2(): both = jnp.concatenate(arrays, axis=along)]
  transfers between devices with their start and end apart: 1 -> 0, of which waited for: 1 -> 0; matrix products, arithmetic and copies ran while one was open for 3% -> 0% of each run, Pallas kernels for 0% -> 0%
where the time goes in v1:
time: 106 us; the launch traced here: 105 us
  Pallas kernels  98.2 us (93%)
  local copies, waits for them, and re-layouts  6.5 us (6%)
    pallas_call x1, Pallas kernels, on_device(): pl.pallas_call(functools.partial(body, nz, scale), out_shape=(jax.ShapeDt...  98.2 us
    unnamed x4, local copies, waits for them, and re-layouts  6.5 us

profile of v1, /device:TPU:32, one launch (start us, length us, event | category | flops | bytes accessed | tf_op | source)
XLA Modules:
  0.0 105.3 jit_solution(18022508435716409305)
XLA Ops:
  0.6 98.2 %shard_map.84 = (bf16[128,2048]{1,0:T(8,128)(2,1)}, f32[32,768]{1,0:T(8,128)}, f32[32,768]{1,0:T(8,128)}, f32[32,768]{1,0:T(8,128)}) custom-call(bf16[128,2048]{1,0:T(8,128)(2,1)} %tok_hbm.1, bf16[128,2048]{1,0:T(8,128)(2,1)} %cot_hbm.1, bf16[2048,768]{1,0:T(8,128)(2,1)} %gw_hbm.1, bf16[2048,768]{1,0:T(8,128)(2,1)} %uw_hbm.1, bf16[2048,768]{1,0:T(8,128)(2,1)} %dw_hbm.1), custom_call_target="tpu_custom_call" | custom-call | tf_op jit(solution)/shard_map/pallas_call | solution.py:402
  98.8 1.9 %copy.13 = bf16[128,2048]{1,0:T(8,128)(2,1)} copy(bf16[128,2048]{1,0:T(8,128)(2,1)} %get-tuple-element.8) | data formatting | bytes 1048576
  100.7 1.5 %copy.14 = f32[32,768]{1,0:T(8,128)} copy(f32[32,768]{1,0:T(8,128)} %get-tuple-element.9) | data formatting | bytes 196608
  102.2 1.5 %copy.15 = f32[32,768]{1,0:T(8,128)} copy(f32[32,768]{1,0:T(8,128)} %get-tuple-element.10) | data formatting | bytes 196608
  103.8 1.5 %copy.16 = f32[32,768]{1,0:T(8,128)} copy(f32[32,768]{1,0:T(8,128)} %get-tuple-element.11) | data formatting | bytes 196608

commit v2 on v1

--- a/solution.py
+++ b/solution.py
@@ -15,7 +15,7 @@
 
 def body(
     nz, scale, tok_hbm, cot_hbm, gw_hbm, uw_hbm, dw_hbm, ig_ref, gg_ref, ug_ref, dg_ref,
-    tok, cot, tokt, cott, gw, uw, dw, gpre, upre, hid, gb, ub, part, xhalf, xfull,
+    tok, cot, tokt, cott, gw, uw, dw, gwt, uwt, gpre, upre, hid, gb, ub, part, xhalf, xfull,
     prod, peer, summed, ya, za, zb, yb,
     ld_sem, ag_s, ag_r, dd_s, dd_r, xs_s, xs_r, rs_s, rs_r,
 ):
@@ -91,53 +91,57 @@
 
     nt = 256
 
+    def rows_of(slot):
+        return pl.ds(pl.multiple_of(slot * rows, rows), rows)
+
     def turned(src, dst, slot):
-        at = pl.ds(pl.multiple_of(slot * rows, rows), rows)
-
+        dst[:, rows_of(slot)] = src[slot].T
+
+    def turn_weights():
         def one(i, _):
-            cols = pl.ds(pl.multiple_of(i * nt, nt), nt)
-            dst[cols, at] = src[slot, :, cols].T
+            lines = pl.ds(pl.multiple_of(i * nt, nt), nt)
+            gwt[:, lines] = gw[lines, :].T
+            uwt[:, lines] = uw[lines, :].T
             return 0
 
         lax.fori_loop(0, d // nt, one, 0)
 
     def forward(slot):
-        def one(i, _):
-            cols = pl.ds(pl.multiple_of(i * nt, nt), nt)
+        at = rows_of(slot)
+
+        def one(i):
+            cols = pl.ds(i * nt, nt)
             g = jnp.dot(tok[slot], gw[:, cols], preferred_element_type=F32)
             u = jnp.dot(tok[slot], uw[:, cols], preferred_element_type=F32)
             gpre[slot, :, cols] = g
             upre[slot, :, cols] = u
-            hid[slot, :, cols] = (g * jax.nn.sigmoid(g) * u).astype(BF16)
-            return 0
-
-        lax.fori_loop(0, ff // nt, one, 0)
+            hid[at, cols] = (g * jax.nn.sigmoid(g) * u).astype(BF16)
+
+        for i in range(ff // nt):
+            one(i)
         turned(tok, tokt, slot)
 
     def backward(slot):
-        def one(i, _):
-            cols = pl.ds(pl.multiple_of(i * nt, nt), nt)
+        at = rows_of(slot)
+
+        def one(i):
+            cols = pl.ds(i * nt, nt)
             h = jnp.dot(cot[slot], dw[:, cols], preferred_element_type=F32)
             g = gpre[slot, :, cols]
             sig = jax.nn.sigmoid(g)
-            gb[slot, :, cols] = (h * upre[slot, :, cols] * sig * (1.0 + g * (1.0 - sig))).astype(BF16)
-            ub[slot, :, cols] = (h * (g * sig)).astype(BF16)
-            return 0
-
-        lax.fori_loop(0, ff // nt, one, 0)
-        turned(cot, cott, slot)
+            gb[at, cols] = (h * upre[slot, :, cols] * sig * (1.0 + g * (1.0 - sig))).astype(BF16)
+            ub[at, cols] = (h * (g * sig)).astype(BF16)
+
+        for i in range(ff // nt):
+            one(i)
 
     def input_part(slot):
-        across = (((1,), (1,)), ((), ()))
-
-        def one(i, _):
-            cols = pl.ds(pl.multiple_of(i * nt, nt), nt)
-            p = lax.dot_general(gb[slot], gw[cols, :], across, preferred_element_type=F32)
-            p += lax.dot_general(ub[slot], uw[cols, :], across, preferred_element_type=F32)
+        at = rows_of(slot)
+        for i in range(d // nt):
+            cols = pl.ds(i * nt, nt)
+            p = jnp.dot(gb[at, :], gwt[:, cols], preferred_element_type=F32)
+            p += jnp.dot(ub[at, :], uwt[:, cols], preferred_element_type=F32)
             part[slot, :, cols] = p.astype(BF16)
-            return 0
-
-        lax.fori_loop(0, d // nt, one, 0)
 
     def x_first(way):
         return remote(
@@ -174,31 +178,28 @@
         lax.fori_loop(0, rows // 16, one, 0)
 
     def pair(k, i):
-        return remote(prod.at[k, i, :, other], peer.at[k, i], dd_s.at[k, i], dd_r.at[k, i], {"tp": other})
-
-    dt = NY * 2 * 32
-
-    def weight_sums(k, left, right):
-        def one(i, _):
-            lines = pl.ds(pl.multiple_of(i * dt, dt), dt)
+        zs = pl.ds(i * zt, zt)
+        return remote(prod.at[k, zs, :, other], peer.at[k, zs], dd_s.at[k, i], dd_r.at[k, i], {"tp": other})
+
+    zt = 2
+    dt = zt * NY * 2 * 32
+
+    def weight_sums(k, left, right, steps):
+        for i in steps:
+            lines = pl.ds(i * dt, dt)
             for j in range(ff // nt):
                 cols = pl.ds(j * nt, nt)
-                acc = jnp.dot(left[lines, 0:rows], right[0, :, cols], preferred_element_type=F32)
-                for s in range(1, nx):
-                    acc += jnp.dot(
-                        left[lines, s * rows : (s + 1) * rows], right[s, :, cols], preferred_element_type=F32
-                    )
-                prod[k, i, :, :, :, cols] = acc.astype(BF16).reshape(NY, 2, 32, nt)
+                acc = jnp.dot(left[lines, :], right[:, cols], preferred_element_type=F32)
+                prod[k, i * zt : (i + 1) * zt, :, :, :, cols] = acc.astype(BF16).reshape(zt, NY, 2, 32, nt)
             pair(k, i).start()
-            return 0
-
-        lax.fori_loop(0, nz, one, 0)
 
     fa = ff // 2
 
     def pair_sum(k):
+        for i in range(nz // zt):
+            pair(k, i).wait_recv()
+
         def one(i, _):
-            pair(k, i).wait_recv()
             for j in range(NY):
                 both = prod[k, i, j, t].astype(F32) + peer[k, i, j].astype(F32)
                 both = both.astype(BF16)
@@ -308,16 +309,19 @@
         elif n == n1 + n2:
             chain_end(k, half_no, second, True)
 
+    early, late = range(nz // zt // 2), range(nz // zt // 2, nz // zt)
     loads[0].wait()
     gather_out(0)
     loads[1].wait()
     loads[2].wait()
     forward(x)
+    turn_weights()
     pass_on(0)
     loads[3].wait()
     gather_out(1)
     loads[4].wait()
     backward(x)
+    turned(cot, cott, x)
     input_part(x)
     gather_in(0, 0, 1)
     forward(prv)
@@ -329,27 +333,33 @@
     pass_on(1)
     gather_in(1, 0, 1)
     backward(prv)
+    turned(cot, cott, prv)
     gather_in(1, 1, 1)
     backward(nxt)
-    input_part(prv)
-    input_part(nxt)
+    turned(cot, cott, nxt)
     gather_in(1, 0, 2)
     gather_in(1, 1, 2)
+    turned(cot, cott, opp)
+    weight_sums(0, cott, hid, early)
+    weight_sums(0, cott, hid, late)
     backward(opp)
-    weight_sums(0, cott, hid)
-    weight_sums(1, tokt, gb)
+    weight_sums(1, tokt, gb, early)
     pair_sum(0)
     stage(0, 0, 0)
     stage(0, 1, 0)
-    weight_sums(2, tokt, ub)
+    weight_sums(1, tokt, gb, late)
+    weight_sums(2, tokt, ub, early)
     pair_sum(1)
     stage(1, 0, 0)
     stage(1, 1, 0)
+    weight_sums(2, tokt, ub, late)
     input_part(opp)
     x_start()
     pair_sum(2)
     stage(2, 0, 0)
     stage(2, 1, 0)
+    input_part(prv)
+    input_part(nxt)
     n_stages = ly[0] + lz[0] + 1
     for n in range(1, n_stages):
         for k in range(3):
@@ -369,18 +379,24 @@
         x_first(way).wait_send()
         x_second(way).wait_send()
 
-    def drain(i, _):
-        for k in range(3):
+    for k in range(3):
+        for i in range(nz // zt):
             pair(k, i).wait_send()
-        return 0
-
-    lax.fori_loop(0, nz, drain, 0)
     for k in range(3):
         for half_no in range(2):
             for axis in range(2):
                 for way in range(2):
                     for step in range((ly, lz)[axis][way]):
                         chain_copy(k, half_no, axis, way, step).wait_send()
+
+
+def written(*refs):
+    n = (len(refs) - 1) // 2
+    copies = [pltpu.make_async_copy(refs[k], refs[n + k], refs[-1].at[k]) for k in range(n)]
+    for copy in copies:
+        copy.start()
+    for copy in copies:
+        copy.wait()
 
 
 def solution(mesh):
@@ -396,12 +412,12 @@
         lines = d // (n_rep * cores)
         fa = ff // 2
         ny_msgs, nz_msgs = NY - 1, nz - 1
-        grad = jax.ShapeDtypeStruct((lines, ff), F32)
+        shapes = (((rows, d), BF16),) + (((lines, ff), F32),) * 3
         vmem = pl.BlockSpec(memory_space=pltpu.VMEM)
         dma = pltpu.SemaphoreType.DMA
-        return pl.pallas_call(
+        results = pl.pallas_call(
             functools.partial(body, nz, scale),
-            out_shape=(jax.ShapeDtypeStruct((rows, d), BF16), grad, grad, grad),
+            out_shape=tuple(pltpu.VMEM(*s) for s in shapes),
             in_specs=[pl.BlockSpec(memory_space=pl.ANY)] * 5,
             out_specs=(vmem,) * 4,
             scratch_shapes=[
@@ -412,11 +428,13 @@
                 pltpu.VMEM((d, ff), BF16),
                 pltpu.VMEM((d, ff), BF16),
                 pltpu.VMEM((d, ff), BF16),
+                pltpu.VMEM((ff, d), BF16),
+                pltpu.VMEM((ff, d), BF16),
                 pltpu.VMEM((nx, rows, ff), F32),
                 pltpu.VMEM((nx, rows, ff), F32),
-                pltpu.VMEM((nx, rows, ff), BF16),
-                pltpu.VMEM((nx, rows, ff), BF16),
-                pltpu.VMEM((nx, rows, ff), BF16),
+                pltpu.VMEM((nx * rows, ff), BF16),
+                pltpu.VMEM((nx * rows, ff), BF16),
+                pltpu.VMEM((nx * rows, ff), BF16),
                 pltpu.VMEM((nx, rows, d), BF16),
                 pltpu.VMEM((2, rows // 2, d), BF16),
                 pltpu.VMEM((2, rows, d), BF16),
@@ -430,17 +448,24 @@
                 dma((5,)),
                 dma((2, 2, 3)),
                 dma((2, 2, 3)),
-                dma((3, nz)),
-                dma((3, nz)),
+                dma((3, nz // 2)),
+                dma((3, nz // 2)),
                 dma((4,)),
                 dma((4,)),
                 dma((3, 2, ny_msgs + nz_msgs)),
                 dma((3, 2, ny_msgs + nz_msgs)),
             ],
             compiler_params=pltpu.CompilerParams(
-                collective_id=0, has_side_effects=True, vmem_limit_bytes=64 * 1024 * 1024 - 128 * 1024
+                collective_id=0, has_side_effects=True, vmem_limit_bytes=60 * 1024 * 1024
             ),
         )(tokens, cotangent, gate_weight, up_weight, down_weight_t)
+        return pl.pallas_call(
+            written,
+            out_shape=tuple(jax.ShapeDtypeStruct(*s) for s in shapes),
+            in_specs=[vmem] * 4,
+            out_specs=(pl.BlockSpec(memory_space=pltpu.HBM),) * 4,
+            scratch_shapes=[dma((4,))],
+        )(*[pltpu.with_memory_space_constraint(r, pltpu.VMEM) for r in results])
 
     return jax.shard_map(
         on_device,

time: 106 us -> 88.6 us (0.84)
  Pallas kernels: 98.2 us -> 87.5 us
  local copies, waits for them, and re-layouts: 6.5 us -> 0 us
    pallas_call x1 -> x2, Pallas kernels: 98.2 us -> 87.5 us  [the longest x1 86.6 us: on_device(): pl.pallas_call(functools.partial(body, nz, scale), out_shape=tuple((pltpu...]
    unnamed x4 -> x0, local copies, waits for them, and re-layouts: 6.5 us -> none
where the time goes in v2:
time: 88.6 us; the launch traced here: 88.3 us
  Pallas kernels  87.5 us (99%)
    pallas_call x1, Pallas kernels, on_device(): pl.pallas_call(functools.partial(body, nz, scale), out_shape=tuple((pltpu...  86.6 us

profile of v2, /device:TPU:32, one launch (start us, length us, event | category | flops | bytes accessed | tf_op | source)
XLA Modules:
  0.0 88.3 jit_solution(5512868028348464056)
XLA Ops:
  0.6 86.6 %shard_map.84 = (bf16[128,2048]{1,0:T(8,128)(2,1)S(1)}, f32[32,768]{1,0:T(8,128)S(1)}, f32[32,768]{1,0:T(8,128)S(1)}, f32[32,768]{1,0:T(8,128)S(1)}) custom-call(bf16[128,2048]{1,0:T(8,128)(2,1)} %tok_hbm.1, bf16[128,2048]{1,0:T(8,128)(2,1)} %cot_hbm.1, bf16[2048,768]{1,0:T(8,128)(2,1)} %gw_hbm.1, bf16[2048,768]{1,0:T(8,128)(2,1)} %uw_hbm.1, ...), custom_call_target="tpu_custom_call" | custom-call | tf_op jit(solution)/shard_map/pallas_call | solution.py:418
  87.2 0.9 %shard_map.85 = (bf16[128,2048]{1,0:T(8,128)(2,1)}, f32[32,768]{1,0:T(8,128)}, f32[32,768]{1,0:T(8,128)}, f32[32,768]{1,0:T(8,128)}) custom-call(bf16[128,2048]{1,0:T(8,128)(2,1)S(1)} %get-tuple-element.8.refs_0_, f32[32,768]{1,0:T(8,128)S(1)} %get-tuple-element.9.refs_1_, f32[32,768]{1,0:T(8,128)S(1)} %get-tuple-element.10.refs_2_, ...), custom_call_target="tpu_custom_call" | custom-call | tf_op jit(solution)/shard_map/pallas_call | solution.py:462

commit v3 on v2

v3 whole, which is shorter than its diff:
```python
import functools

import jax
import jax.numpy as jnp
from jax import lax
from jax.experimental import pallas as pl
from jax.experimental.pallas import tpu as pltpu
from jax.sharding import PartitionSpec as P

MESH = pl.DeviceIdType.MESH
F32 = jnp.float32
BF16 = jnp.bfloat16
NY = 4
WIDTH_A = (384, 384, 512)


def body(
    nz, scale, tok_hbm, cot_hbm, gw_hbm, uw_hbm, dw_hbm, ig_ref, gg_ref, ug_ref, dg_ref,
    tok, cot, tokt, cott, gw, uw, dw, gwt, uwt, gpre, upre, hpre, hid, gb, ub, part, xhalf, xfull,
    prod, peer, *rest,
):
    sa, sb, ya, za, zb, yb = (rest[3 * i : 3 * i + 3] for i in range(6))
    ld_sem, ag_s, ag_r, dd_s, dd_r, xs_s, xs_r, rs_s, rs_r = rest[18:]
    rep = lax.axis_index("rep")
    x = lax.axis_index("fs")
    t = lax.axis_index("tp")
    nx = 4
    rows = tok.shape[1]
    half = rows // 2
    d, ff = gw.shape
    hd = d // 2
    zw = d // nz
    hz = nz // 2
    z = rep // NY
    y = lax.rem(rep, NY)
    nxt, prv, opp = lax.rem(x + 1, nx), lax.rem(x + nx - 1, nx), lax.rem(x + 2, nx)
    other = 1 - t
    sgn = 1 - 2 * t

    def along_y(step):
        return lax.rem(y + NY + step, NY)

    def along_z(step):
        return lax.rem(z + nz + step, nz)

    def place(zi):
        return zi % 2 * hz + zi // 2 if isinstance(zi, int) else lax.rem(zi, 2) * hz + zi // 2

    def dev_y(step):
        return {"rep": z * NY + along_y(step)}

    def dev_z(step):
        return {"rep": along_z(step) * NY + y}

    def on_parity(e, yes, no=None):
        mine = lax.rem(z, 2) == e
        pl.when(mine)(yes)
        if no is not None:
            pl.when(jnp.logical_not(mine))(no)

    parts = [(tok_hbm, tok.at[x]), (gw_hbm, gw), (uw_hbm, uw)]
    for zi in range(nz):
        cols = pl.ds(zi * zw, zw)
        parts.append((cot_hbm.at[:, cols], cot.at[zi % 2, x, :, pl.ds(zi // 2 * zw, zw)]))
    for zi in range(nz):
        parts.append((dw_hbm.at[pl.ds(zi * zw, zw), :], dw.at[pl.ds(place(zi) * zw, zw), :]))
    loads = [pltpu.make_async_copy(src, dst, ld_sem.at[k]) for k, (src, dst) in enumerate(parts)]
    for load in loads:
        load.start()

    barrier = pltpu.get_barrier_semaphore()
    peers = [{"fs": nxt}, {"fs": prv}, {"tp": other}]
    peers += [dev_y(s) for s in (1, -1, 2)] + [dev_z(s) for s in (1, -1, 2, -2)]
    for who in peers:
        pl.semaphore_signal(barrier, inc=1, device_id=who, device_id_type=MESH)
    pl.semaphore_wait(barrier, len(peers))

    def remote(src, dst, s, r, who):
        return pltpu.make_async_remote_copy(
            src_ref=src, dst_ref=dst, send_sem=s, recv_sem=r, device_id=who, device_id_type=MESH
        )

    bufs = (tok, cot.at[0], cot.at[1])
    to = ({"fs": nxt}, {"fs": prv})
    came = (prv, nxt)

    def gather(a, way, k, slot, h):
        ref = bufs[a].at[slot, pl.ds(h * half, half), :]
        return remote(ref, ref, ag_s.at[a, way, k], ag_r.at[a, way, k], to[way])

    def gather_out(a):
        for k in range(2):
            for way in range(2):
                gather(a, way, k, x, k if way == 0 else 1 - k).start()

    def gather_in(a, way, k):
        if k == 2:
            gather(a, way, 2, opp, way).wait_recv()
        else:
            gather(a, way, k, came[way], k if way == 0 else 1 - k).wait_recv()

    def pass_on(a):
        for way in range(2):
            gather_in(a, way, 0)
            gather(a, way, 2, came[way], way).start()

    nt = 256

    def rows_of(slot):
        return pl.ds(pl.multiple_of(slot * rows, rows), rows)

    def turned_cot(e, slot):
        cott[e * hd : (e + 1) * hd, rows_of(slot)] = cot[e, slot].T

    def turn_weights():
        def one(i, _):
            lines = pl.ds(pl.multiple_of(i * nt, nt), nt)
            gwt[:, lines] = gw[lines, :].T
            uwt[:, lines] = uw[lines, :].T
            return 0

        lax.fori_loop(0, d // nt, one, 0)

    def forward(slot):
        at = rows_of(slot)
        for i in range(ff // nt):
            cols = pl.ds(i * nt, nt)
            g = jnp.dot(tok[slot], gw[:, cols], preferred_element_type=F32)
            u = jnp.dot(tok[slot], uw[:, cols], preferred_element_type=F32)
            gpre[slot, :, cols] = g
            upre[slot, :, cols] = u
            hid[at, cols] = (g * jax.nn.sigmoid(g) * u).astype(BF16)
        for zi in range(nz):
            tokt[place(zi) * zw : (place(zi) + 1) * zw, at] = tok[slot, :, zi * zw : (zi + 1) * zw].T

    def hid_part(slot):
        for i in range(ff // nt):
            cols = pl.ds(i * nt, nt)
            hpre[slot, :, cols] = jnp.dot(cot[0, slot], dw[0:hd, cols], preferred_element_type=F32)

    def backward(slot):
        at = rows_of(slot)
        for i in range(ff // nt):
            cols = pl.ds(i * nt, nt)
            h = hpre[slot, :, cols] + jnp.dot(cot[1, slot], dw[hd:d, cols], preferred_element_type=F32)
            g = gpre[slot, :, cols]
            sig = jax.nn.sigmoid(g)
            gb[at, cols] = (h * upre[slot, :, cols] * sig * (1.0 + g * (1.0 - sig))).astype(BF16)
            ub[at, cols] = (h * (g * sig)).astype(BF16)

    def input_part(slot):
        at = rows_of(slot)
        for i in range(d // nt):
            cols = pl.ds(i * nt, nt)
            p = jnp.dot(gb[at, :], gwt[:, cols], preferred_element_type=F32)
            p += jnp.dot(ub[at, :], uwt[:, cols], preferred_element_type=F32)
            part[slot, :, cols] = p.astype(BF16)

    def x_first(way):
        return remote(
            part.at[opp, pl.ds(way * half, half), :], xhalf.at[way], xs_s.at[way], xs_r.at[way], to[way]
        )

    def x_second(way):
        return remote(part.at[(nxt, prv)[way]], xfull.at[way], xs_s.at[2 + way], xs_r.at[2 + way], to[way])

    def x_start():
        for way in range(2):
            x_first(way).start()

    def x_forward():
        for way in range(2):
            x_first(way).wait_recv()
            slot = (nxt, prv)[way]
            for i in range(half // 16):
                at = pl.ds(way * half + i * 16, 16)
                got = xhalf[way, pl.ds(i * 16, 16), :].astype(F32)
                part[slot, at, :] = (part[slot, at, :].astype(F32) + got).astype(BF16)
            x_second(way).start()

    def x_finish():
        for way in range(2):
            x_second(way).wait_recv()

        def one(i, _):
            at = pl.ds(pl.multiple_of(i * 16, 16), 16)
            total = part[x, at, :].astype(F32) + xfull[0, at, :].astype(F32) + xfull[1, at, :].astype(F32)
            ig_ref[at, :] = total.astype(BF16)
            return 0

        lax.fori_loop(0, rows // 16, one, 0)

    zt = 2

    def pair(k, i):
        at = pl.ds(i * zt, zt)
        return remote(prod.at[k, at, :, other], peer.at[k, at], dd_s.at[k, i], dd_r.at[k, i], {"tp": other})

    left, right, outs = (cott, tokt, tokt), (hid, gb, ub), (dg_ref, gg_ref, ug_ref)

    def weight_sums(k, e):
        for i in range(e * hz // zt, (e + 1) * hz // zt):
            lines = pl.ds(i * zt * zw, zt * zw)
            for j in range(ff // nt):
                cols = pl.ds(j * nt, nt)
                acc = jnp.dot(left[k][lines, :], right[k][:, cols], preferred_element_type=F32)
                prod[k, i * zt : (i + 1) * zt, :, :, :, cols] = acc.astype(BF16).reshape(zt, NY, 2, 32, nt)
            pair(k, i).start()

    def pair_sum(k, e):
        for i in range(e * hz // zt, (e + 1) * hz // zt):
            pair(k, i).wait_recv()
        wa = WIDTH_A[k]

        def one(i, _):
            for j in range(NY):
                both = prod[k, i, j, t].astype(F32) + peer[k, i, j].astype(F32)
                both = both.astype(BF16)
                sa[k][i, j] = both[:, :wa]
                sb[k][i, j] = both[:, wa:]
            return 0

        lax.fori_loop(e * hz, (e + 1) * hz, one, 0)

    ly, lz = (2, 1), (4, 3)

    def sems(k, e, h, n):
        u = (k * 2 + e) * 2 + h
        return rs_s.at[u, n], rs_r.at[u, n]

    def go(way):
        return sgn if way == 0 else -sgn

    def a_y(k, e, way, step):
        m = step if way == 0 else 2
        at = pl.ds(e * hz, hz)
        dest = along_y((ly[way] - step) * go(way))
        return remote(sa[k].at[at, dest], ya[k].at[m, at], *sems(k, e, 0, m), dev_y(go(way)))

    hops = {"a": (4, 2), "b": (3, 1), "c": (1, 1), "d": (2, 2), "e": (-3, -2), "f": (-2, -1), "g": (-1, -1)}

    def a_z(k, e, name):
        m = "abcdefg".index(name)
        owner, target = hops[name]
        src = sa[k].at[place(along_z(owner * sgn)), y]
        return remote(src, za[k].at[m], *sems(k, e, 0, 3 + m), dev_z(target * sgn))

    def b_z(k, e, way, step):
        m = step if way == 0 else lz[0] + step
        src = sb[k].at[place(along_z((lz[way] - step) * go(way)))]
        return remote(src, zb[k].at[m], *sems(k, e, 1, m), dev_z(go(way)))

    y_steps = (1, -1, 2)

    def b_y(k, e, m):
        src = sb[k].at[place(z), along_y(y_steps[m])]
        return remote(src, yb[k].at[m], *sems(k, e, 1, 7 + m), dev_y(y_steps[m]))

    def added(ref, at, arrived):
        v = ref[at].astype(F32)
        for got in arrived:
            v += got.astype(F32)
        return v

    def a_stage(k, e, n):
        names = "abcdefg"
        if n <= 1:
            for way in range(2):
                if n >= ly[way]:
                    continue
                if n == 1:
                    a_y(k, e, way, 0).wait_recv()
                    at = along_y((ly[way] - 1) * go(way))
                    for i in range(e * hz, (e + 1) * hz):
                        sa[k][i, at] = added(sa[k], (i, at), [ya[k][0, i]]).astype(BF16)
                a_y(k, e, way, n).start()
        elif n == 2:
            a_y(k, e, 0, 1).wait_recv()
            a_y(k, e, 1, 0).wait_recv()
            for i in range(e * hz, (e + 1) * hz):
                sa[k][i, y] = added(sa[k], (i, y), [ya[k][1, i], ya[k][2, i]]).astype(BF16)

            def yes():
                for name in "af":
                    a_z(k, e, name).start()

            def no():
                for name in "ecb":
                    a_z(k, e, name).start()

            on_parity(e, yes, no)
        elif n == 3:

            def relay(one, two, step, out):
                a_z(k, e, one).wait_recv()
                a_z(k, e, two).wait_recv()
                at = (place(along_z(step * sgn)), y)
                got = [za[k][names.index(one)], za[k][names.index(two)]]
                sa[k][at] = added(sa[k], at, got).astype(BF16)
                a_z(k, e, out).start()

            on_parity(e, lambda: relay("a", "b", 2, "d"), lambda: relay("e", "f", -1, "g"))
        else:

            def end():
                for name in "cdg":
                    a_z(k, e, name).wait_recv()
                v = added(sa[k], (place(z), y), [za[k][names.index(c)] for c in "cdg"])
                outs[k][:, : WIDTH_A[k]] = v * scale

            on_parity(e, end)

    def b_sum(k, at, ms):
        for j in range(NY):
            sb[k][at, j] = added(sb[k], (at, j), [zb[k][m, j] for m in ms]).astype(BF16)

    def b_stage(k, e, n):
        if n <= 3:

            def step(way):
                if n > 0:
                    b_z(k, e, way, n - 1).wait_recv()
                    m = n - 1 if way == 0 else lz[0] + n - 1
                    b_sum(k, place(along_z((lz[way] - n) * go(way))), [m])
                b_z(k, e, way, n).start()

            def steps(rest_of):
                def run():
                    for way in range(2):
                        if n < lz[way] and (lz[way] - n) % 2 == rest_of:
                            step(way)

                return run

            on_parity(e, steps(0), steps(1))
        elif n == 4:

            def turn():
                b_z(k, e, 0, 3).wait_recv()
                b_z(k, e, 1, 2).wait_recv()
                b_sum(k, place(z), [3, 6])
                for m in range(3):
                    b_y(k, e, m).start()

            on_parity(e, turn)
        else:

            def end():
                for m in range(3):
                    b_y(k, e, m).wait_recv()
                v = added(sb[k], (place(z), y), [yb[k][m] for m in range(3)])
                outs[k][:, WIDTH_A[k] :] = v * scale

            on_parity(e, end)

    def stage(k, e, h, n):
        (a_stage, b_stage)[h](k, e, n)

    loads[0].wait()
    gather_out(0)
    loads[1].wait()
    loads[2].wait()
    forward(x)
    turn_weights()
    pass_on(0)
    for load in loads[3 : 3 + nz]:
        load.wait()
    gather_out(1)
    for load in loads[3 + nz :]:
        load.wait()
    hid_part(x)
    turned_cot(0, x)
    backward(x)
    turned_cot(1, x)
    input_part(x)
    gather_in(0, 0, 1)
    forward(prv)
    gather_in(0, 1, 1)
    forward(nxt)
    gather_in(0, 0, 2)
    gather_in(0, 1, 2)
    forward(opp)
    pass_on(1)
    gather_out(2)
    gather_in(1, 0, 1)
    hid_part(prv)
    turned_cot(0, prv)
    gather_in(1, 1, 1)
    hid_part(nxt)
    turned_cot(0, nxt)
    gather_in(1, 0, 2)
    gather_in(1, 1, 2)
    turned_cot(0, opp)
    weight_sums(0, 0)
    hid_part(opp)
    pair_sum(0, 0)
    stage(0, 0, 1, 0)
    stage(0, 0, 0, 0)
    pass_on(2)
    gather_in(2, 0, 1)
    gather_in(2, 1, 1)
    backward(prv)
    stage(0, 0, 1, 1)
    backward(nxt)
    turned_cot(1, prv)
    turned_cot(1, nxt)
    stage(0, 0, 0, 1)
    gather_in(2, 0, 2)
    gather_in(2, 1, 2)
    turned_cot(1, opp)
    weight_sums(0, 1)
    stage(0, 0, 1, 2)
    backward(opp)
    weight_sums(1, 0)
    stage(0, 0, 0, 2)
    pair_sum(0, 1)
    stage(0, 1, 1, 0)
    stage(0, 1, 0, 0)
    weight_sums(1, 1)
    stage(0, 0, 1, 3)
    pair_sum(1, 0)
    stage(1, 0, 1, 0)
    stage(1, 0, 0, 0)
    weight_sums(2, 0)
    pair_sum(1, 1)
    stage(1, 1, 1, 0)
    stage(1, 1, 0, 0)
    stage(0, 0, 0, 3)
    weight_sums(2, 1)
    stage(0, 1, 1, 1)
    stage(0, 1, 0, 1)
    stage(0, 0, 1, 4)
    pair_sum(2, 0)
    stage(2, 0, 1, 0)
    stage(2, 0, 0, 0)
    stage(1, 0, 1, 1)
    input_part(opp)
    stage(1, 0, 0, 1)
    pair_sum(2, 1)
    stage(2, 1, 1, 0)
    stage(2, 1, 0, 0)
    stage(1, 1, 1, 1)
    x_start()
    input_part(prv)
    stage(0, 0, 0, 4)
    input_part(nxt)
    stage(1, 1, 0, 1)
    stage(2, 0, 1, 1)
    stage(0, 1, 1, 2)
    stage(1, 0, 1, 2)
    stage(0, 1, 0, 2)
    stage(2, 1, 1, 1)
    stage(0, 0, 1, 5)
    stage(1, 1, 1, 2)
    stage(2, 0, 1, 2)
    stage(0, 1, 1, 3)
    stage(2, 0, 0, 1)
    stage(1, 0, 1, 3)
    x_forward()
    stage(1, 0, 0, 2)
    stage(0, 1, 0, 3)
    stage(2, 1, 1, 2)
    stage(2, 1, 0, 1)
    stage(1, 1, 1, 3)
    stage(1, 1, 0, 2)
    stage(2, 0, 1, 3)
    stage(2, 0, 0, 2)
    stage(0, 1, 1, 4)
    stage(1, 0, 1, 4)
    stage(2, 1, 0, 2)
    stage(1, 0, 0, 3)
    stage(2, 1, 1, 3)
    stage(0, 1, 0, 4)
    stage(0, 1, 1, 5)
    stage(1, 1, 1, 4)
    stage(1, 0, 1, 5)
    stage(1, 1, 0, 3)
    stage(2, 0, 1, 4)
    stage(2, 0, 0, 3)
    stage(1, 1, 1, 5)
    stage(2, 1, 0, 3)
    stage(2, 1, 1, 4)
    stage(1, 0, 0, 4)
    stage(2, 0, 1, 5)
    stage(1, 1, 0, 4)
    x_finish()
    stage(2, 0, 0, 4)
    stage(2, 1, 1, 5)
    stage(2, 1, 0, 4)

    for a in range(3):
        for way in range(2):
            for k in range(2):
                gather(a, way, k, x, k if way == 0 else 1 - k).wait_send()
            gather(a, way, 2, came[way], way).wait_send()
    for way in range(2):
        x_first(way).wait_send()
        x_second(way).wait_send()
    for k in range(3):
        for i in range(nz // zt):
            pair(k, i).wait_send()
        for e in range(2):
            for way, step in ((0, 0), (0, 1), (1, 0)):
                a_y(k, e, way, step).wait_send()

    def sent(k, e, names, steps, direct):
        for name in names:
            a_z(k, e, name).wait_send()
        for way, step in steps:
            b_z(k, e, way, step).wait_send()
        for m in direct:
            b_y(k, e, m).wait_send()

    for e in range(2):

        def yes():
            for k in range(3):
                sent(k, e, "afd", ((0, 0), (0, 2), (1, 1)), range(3))

        def no():
            for k in range(3):
                sent(k, e, "bceg", ((0, 1), (0, 3), (1, 0), (1, 2)), ())

        on_parity(e, yes, no)


def written(*refs):
    n = (len(refs) - 1) // 2
    copies = [pltpu.make_async_copy(refs[k], refs[n + k], refs[-1].at[k]) for k in range(n)]
    for copy in copies:
        copy.start()
    for copy in copies:
        copy.wait()


def solution(mesh):
    n_rep = mesh.shape["rep"]
    nz = n_rep // NY
    nx = mesh.shape["fs"]
    cores = mesh.shape["tp"]

    def on_device(tokens, cotangent, gate_weight, up_weight, down_weight_t):
        rows, d = tokens.shape
        ff = gate_weight.shape[1]
        scale = float(rows * n_rep * nx * cores) ** (-0.5)
        lines = d // (n_rep * cores)
        wb = tuple(ff - w for w in WIDTH_A)
        shapes = (((rows, d), BF16),) + (((lines, ff), F32),) * 3
        vmem = pl.BlockSpec(memory_space=pltpu.VMEM)
        dma = pltpu.SemaphoreType.DMA
        results = pl.pallas_call(
            functools.partial(body, nz, scale),
            out_shape=tuple(pltpu.VMEM(*s) for s in shapes),
            in_specs=[pl.BlockSpec(memory_space=pl.ANY)] * 5,
            out_specs=(vmem,) * 4,
            scratch_shapes=[
                pltpu.VMEM((nx, rows, d), BF16),
                pltpu.VMEM((2, nx, rows, d // 2), BF16),
                pltpu.VMEM((d, nx * rows), BF16),
                pltpu.VMEM((d, nx * rows), BF16),
                pltpu.VMEM((d, ff), BF16),
                pltpu.VMEM((d, ff), BF16),
                pltpu.VMEM((d, ff), BF16),
                pltpu.VMEM((ff, d), BF16),
                pltpu.VMEM((ff, d), BF16),
                pltpu.VMEM((nx, rows, ff), F32),
                pltpu.VMEM((nx, rows, ff), F32),
                pltpu.VMEM((nx, rows, ff), F32),
                pltpu.VMEM((nx * rows, ff), BF16),
                pltpu.VMEM((nx * rows, ff), BF16),
                pltpu.VMEM((nx * rows, ff), BF16),
                pltpu.VMEM((nx, rows, d), BF16),
                pltpu.VMEM((2, rows // 2, d), BF16),
                pltpu.VMEM((2, rows, d), BF16),
                pltpu.VMEM((3, nz, NY, cores, lines, ff), BF16),
                pltpu.VMEM((3, nz, NY, lines, ff), BF16),
                *[pltpu.VMEM((nz, NY, lines, w), BF16) for w in WIDTH_A],
                *[pltpu.VMEM((nz, NY, lines, w), BF16) for w in wb],
                *[pltpu.VMEM((3, nz, lines, w), BF16) for w in WIDTH_A],
                *[pltpu.VMEM((7, lines, w), BF16) for w in WIDTH_A],
                *[pltpu.VMEM((7, NY, lines, w), BF16) for w in wb],
                *[pltpu.VMEM((3, lines, w), BF16) for w in wb],
                dma((3 + 2 * nz,)),
                dma((3, 2, 3)),
                dma((3, 2, 3)),
                dma((3, nz // 2)),
                dma((3, nz // 2)),
                dma((4,)),
                dma((4,)),
                dma((12, 10)),
                dma((12, 10)),
            ],
            compiler_params=pltpu.CompilerParams(
                collective_id=0, has_side_effects=True, vmem_limit_bytes=60 * 1024 * 1024
            ),
        )(tokens, cotangent, gate_weight, up_weight, down_weight_t)
        return pl.pallas_call(
            written,
            out_shape=tuple(jax.ShapeDtypeStruct(*s) for s in shapes),
            in_specs=[vmem] * 4,
            out_specs=(pl.BlockSpec(memory_space=pltpu.HBM),) * 4,
            scratch_shapes=[dma((4,))],
        )(*[pltpu.with_memory_space_constraint(r, pltpu.VMEM) for r in results])

    return jax.shard_map(
        on_device,
        mesh=mesh,
        in_specs=(
            P(("rep", "fs", "tp"), None),
            P(("rep", "fs", "tp"), None),
            P(None, "fs"),
            P(None, "fs"),
            P(None, "fs"),
        ),
        out_specs=(
            P(("rep", "fs", "tp"), None),
            P(("rep", "tp"), "fs"),
            P(("rep", "tp"), "fs"),
            P(("rep", "tp"), "fs"),
        ),
        check_vma=False,
    )
```

time: 88.6 us -> 88 us (level)
  no operation moved by 1% of the time
where the time goes in v3:
time: 88 us
  Pallas kernels  87.2 us (99%)
    pallas_call x1, Pallas kernels, on_device(): pl.pallas_call(functools.partial(body, nz, scale), out_shape=tuple((pltpu...  86.3 us

profile of v3, /device:TPU:32, one launch (start us, length us, event | category | flops | bytes accessed | tf_op | source)
XLA Modules:
  0.0 88.0 jit_solution(516553929371474812)
XLA Ops:
  0.6 86.3 %shard_map.84 = (bf16[128,2048]{1,0:T(8,128)(2,1)S(1)}, f32[32,768]{1,0:T(8,128)S(1)}, f32[32,768]{1,0:T(8,128)S(1)}, f32[32,768]{1,0:T(8,128)S(1)}) custom-call(bf16[128,2048]{1,0:T(8,128)(2,1)} %tok_hbm.1, bf16[128,2048]{1,0:T(8,128)(2,1)} %cot_hbm.1, bf16[2048,768]{1,0:T(8,128)(2,1)} %gw_hbm.1, bf16[2048,768]{1,0:T(8,128)(2,1)} %uw_hbm.1, ...), custom_call_target="tpu_custom_call" | custom-call | tf_op jit(solution)/shard_map/pallas_call | solution.py:551
  86.9 0.9 %shard_map.85 = (bf16[128,2048]{1,0:T(8,128)(2,1)}, f32[32,768]{1,0:T(8,128)}, f32[32,768]{1,0:T(8,128)}, f32[32,768]{1,0:T(8,128)}) custom-call(bf16[128,2048]{1,0:T(8,128)(2,1)S(1)} %get-tuple-element.8.refs_0_, f32[32,768]{1,0:T(8,128)S(1)} %get-tuple-element.9.refs_1_, f32[32,768]{1,0:T(8,128)S(1)} %get-tuple-element.10.refs_2_, ...), custom_call_target="tpu_custom_call" | custom-call | tf_op jit(solution)/shard_map/pallas_call | solution.py:597

commit v4 on v3

--- a/solution.py
+++ b/solution.py
@@ -11,7 +11,7 @@
 F32 = jnp.float32
 BF16 = jnp.bfloat16
 NY = 4
-WIDTH_A = (384, 384, 512)
+WIDTH_A = (384, 384, 640)
 
 
 def body(
@@ -392,100 +392,100 @@
     gather_in(1, 1, 2)
     turned_cot(0, opp)
     weight_sums(0, 0)
-    hid_part(opp)
+    pass_on(2)
     pair_sum(0, 0)
+    stage(0, 0, 0, 0)
     stage(0, 0, 1, 0)
-    stage(0, 0, 0, 0)
-    pass_on(2)
     gather_in(2, 0, 1)
     gather_in(2, 1, 1)
+    backward(nxt)
+    turned_cot(1, nxt)
     backward(prv)
+    turned_cot(1, prv)
+    hid_part(opp)
     stage(0, 0, 1, 1)
-    backward(nxt)
-    turned_cot(1, prv)
-    turned_cot(1, nxt)
-    stage(0, 0, 0, 1)
     gather_in(2, 0, 2)
     gather_in(2, 1, 2)
     turned_cot(1, opp)
     weight_sums(0, 1)
-    stage(0, 0, 1, 2)
     backward(opp)
+    stage(0, 0, 0, 1)
     weight_sums(1, 0)
-    stage(0, 0, 0, 2)
     pair_sum(0, 1)
+    stage(0, 1, 0, 0)
     stage(0, 1, 1, 0)
-    stage(0, 1, 0, 0)
     weight_sums(1, 1)
-    stage(0, 0, 1, 3)
     pair_sum(1, 0)
     stage(1, 0, 1, 0)
     stage(1, 0, 0, 0)
+    stage(0, 0, 1, 2)
     weight_sums(2, 0)
     pair_sum(1, 1)
+    stage(1, 1, 0, 0)
     stage(1, 1, 1, 0)
-    stage(1, 1, 0, 0)
-    stage(0, 0, 0, 3)
     weight_sums(2, 1)
+    stage(0, 0, 0, 2)
     stage(0, 1, 1, 1)
-    stage(0, 1, 0, 1)
-    stage(0, 0, 1, 4)
     pair_sum(2, 0)
+    input_part(opp)
     stage(2, 0, 1, 0)
     stage(2, 0, 0, 0)
+    stage(1, 1, 1, 1)
+    pair_sum(2, 1)
     stage(1, 0, 1, 1)
-    input_part(opp)
+    stage(0, 0, 1, 3)
+    x_start()
+    stage(1, 1, 0, 1)
+    stage(2, 1, 1, 0)
+    stage(2, 0, 1, 1)
+    stage(0, 1, 0, 1)
+    stage(0, 1, 1, 2)
+    input_part(prv)
+    stage(2, 1, 0, 0)
     stage(1, 0, 0, 1)
-    pair_sum(2, 1)
-    stage(2, 1, 1, 0)
-    stage(2, 1, 0, 0)
-    stage(1, 1, 1, 1)
-    x_start()
-    input_part(prv)
-    stage(0, 0, 0, 4)
     input_part(nxt)
-    stage(1, 1, 0, 1)
-    stage(2, 0, 1, 1)
-    stage(0, 1, 1, 2)
     stage(1, 0, 1, 2)
+    stage(0, 0, 0, 3)
+    stage(1, 1, 1, 2)
+    stage(2, 1, 1, 1)
+    stage(2, 0, 1, 2)
+    stage(2, 0, 0, 1)
+    stage(1, 1, 0, 2)
+    stage(0, 1, 1, 3)
+    stage(1, 0, 1, 3)
     stage(0, 1, 0, 2)
-    stage(2, 1, 1, 1)
-    stage(0, 0, 1, 5)
-    stage(1, 1, 1, 2)
-    stage(2, 0, 1, 2)
-    stage(0, 1, 1, 3)
-    stage(2, 0, 0, 1)
-    stage(1, 0, 1, 3)
     x_forward()
-    stage(1, 0, 0, 2)
-    stage(0, 1, 0, 3)
     stage(2, 1, 1, 2)
     stage(2, 1, 0, 1)
     stage(1, 1, 1, 3)
-    stage(1, 1, 0, 2)
     stage(2, 0, 1, 3)
+    stage(1, 0, 0, 2)
     stage(2, 0, 0, 2)
+    stage(1, 0, 1, 4)
+    stage(2, 1, 1, 3)
+    stage(2, 1, 0, 2)
+    stage(0, 1, 0, 3)
+    stage(2, 1, 1, 4)
     stage(0, 1, 1, 4)
-    stage(1, 0, 1, 4)
-    stage(2, 1, 0, 2)
+    stage(1, 0, 1, 5)
+    stage(2, 0, 0, 3)
+    stage(1, 1, 1, 4)
+    stage(1, 1, 0, 3)
+    stage(0, 0, 1, 4)
     stage(1, 0, 0, 3)
-    stage(2, 1, 1, 3)
+    stage(2, 0, 1, 4)
+    stage(2, 1, 0, 3)
+    stage(2, 1, 1, 5)
+    x_finish()
+    stage(0, 0, 0, 4)
+    stage(2, 0, 0, 4)
+    stage(2, 0, 1, 5)
+    stage(0, 0, 1, 5)
+    stage(1, 1, 1, 5)
+    stage(1, 1, 0, 4)
+    stage(1, 0, 0, 4)
+    stage(0, 1, 1, 5)
     stage(0, 1, 0, 4)
-    stage(0, 1, 1, 5)
-    stage(1, 1, 1, 4)
-    stage(1, 0, 1, 5)
-    stage(1, 1, 0, 3)
-    stage(2, 0, 1, 4)
-    stage(2, 0, 0, 3)
-    stage(1, 1, 1, 5)
-    stage(2, 1, 0, 3)
-    stage(2, 1, 1, 4)
-    stage(1, 0, 0, 4)
-    stage(2, 0, 1, 5)
-    stage(1, 1, 0, 4)
-    x_finish()
-    stage(2, 0, 0, 4)
-    stage(2, 1, 1, 5)
     stage(2, 1, 0, 4)
 
     for a in range(3):

time: 88 us -> 83.1 us (0.944)
  Pallas kernels: 87.2 us -> 82.2 us
    pallas_call x1, Pallas kernels: 86.3 us -> 81.3 us  [on_device(): pl.pallas_call(functools.partial(body, nz, scale), out_shape=tuple((pltpu...]
where the time goes in v4:
time: 83.1 us; the launch traced here: 83 us
  Pallas kernels  82.2 us (99%)
    pallas_call x1, Pallas kernels, on_device(): pl.pallas_call(functools.partial(body, nz, scale), out_shape=tuple((pltpu...  81.3 us

profile of v4, /device:TPU:32, one launch (start us, length us, event | category | flops | bytes accessed | tf_op | source)
XLA Modules:
  0.0 83.0 jit_solution(12403695570530269698)
XLA Ops:
  0.6 81.3 %shard_map.84 = (bf16[128,2048]{1,0:T(8,128)(2,1)S(1)}, f32[32,768]{1,0:T(8,128)S(1)}, f32[32,768]{1,0:T(8,128)S(1)}, f32[32,768]{1,0:T(8,128)S(1)}) custom-call(bf16[128,2048]{1,0:T(8,128)(2,1)} %tok_hbm.1, bf16[128,2048]{1,0:T(8,128)(2,1)} %cot_hbm.1, bf16[2048,768]{1,0:T(8,128)(2,1)} %gw_hbm.1, bf16[2048,768]{1,0:T(8,128)(2,1)} %uw_hbm.1, ...), custom_call_target="tpu_custom_call" | custom-call | tf_op jit(solution)/shard_map/pallas_call | solution.py:551
  82.0 0.9 %shard_map.85 = (bf16[128,2048]{1,0:T(8,128)(2,1)}, f32[32,768]{1,0:T(8,128)}, f32[32,768]{1,0:T(8,128)}, f32[32,768]{1,0:T(8,128)}) custom-call(bf16[128,2048]{1,0:T(8,128)(2,1)S(1)} %get-tuple-element.8.refs_0_, f32[32,768]{1,0:T(8,128)S(1)} %get-tuple-element.9.refs_1_, f32[32,768]{1,0:T(8,128)S(1)} %get-tuple-element.10.refs_2_, ...), custom_call_target="tpu_custom_call" | custom-call | tf_op jit(solution)/shard_map/pallas_call | solution.py:597

commit v5 on v4

--- a/solution.py
+++ b/solution.py
@@ -11,7 +11,9 @@
 F32 = jnp.float32
 BF16 = jnp.bfloat16
 NY = 4
-WIDTH_A = (384, 384, 640)
+WIDTH_A = (384, 384, 512)
+CHAINED = (0, 1)
+OWN, NXT, PRV, OPP = range(4)
 
 
 def body(
@@ -33,7 +35,7 @@
     hz = nz // 2
     z = rep // NY
     y = lax.rem(rep, NY)
-    nxt, prv, opp = lax.rem(x + 1, nx), lax.rem(x + nx - 1, nx), lax.rem(x + 2, nx)
+    nxt, prv = lax.rem(x + 1, nx), lax.rem(x + nx - 1, nx)
     other = 1 - t
     sgn = 1 - 2 * t
 
@@ -58,10 +60,10 @@
         if no is not None:
             pl.when(jnp.logical_not(mine))(no)
 
-    parts = [(tok_hbm, tok.at[x]), (gw_hbm, gw), (uw_hbm, uw)]
+    parts = [(tok_hbm, tok.at[OWN]), (gw_hbm, gw), (uw_hbm, uw)]
     for zi in range(nz):
         cols = pl.ds(zi * zw, zw)
-        parts.append((cot_hbm.at[:, cols], cot.at[zi % 2, x, :, pl.ds(zi // 2 * zw, zw)]))
+        parts.append((cot_hbm.at[:, cols], cot.at[zi % 2, OWN, :, pl.ds(zi // 2 * zw, zw)]))
     for zi in range(nz):
         parts.append((dw_hbm.at[pl.ds(zi * zw, zw), :], dw.at[pl.ds(place(zi) * zw, zw), :]))
     loads = [pltpu.make_async_copy(src, dst, ld_sem.at[k]) for k, (src, dst) in enumerate(parts)]
@@ -82,32 +84,33 @@
 
     bufs = (tok, cot.at[0], cot.at[1])
     to = ({"fs": nxt}, {"fs": prv})
-    came = (prv, nxt)
-
-    def gather(a, way, k, slot, h):
-        ref = bufs[a].at[slot, pl.ds(h * half, half), :]
-        return remote(ref, ref, ag_s.at[a, way, k], ag_r.at[a, way, k], to[way])
+    came = (PRV, NXT)
+
+    def gather(a, way, k):
+        h = way if k == 2 else (k if way == 0 else 1 - k)
+        at = pl.ds(h * half, half)
+        src, dst = (came[way], OPP) if k == 2 else (OWN, came[way])
+        return remote(
+            bufs[a].at[src, at, :], bufs[a].at[dst, at, :], ag_s.at[a, way, k], ag_r.at[a, way, k], to[way]
+        )
 
     def gather_out(a):
         for k in range(2):
             for way in range(2):
-                gather(a, way, k, x, k if way == 0 else 1 - k).start()
+                gather(a, way, k).start()
 
     def gather_in(a, way, k):
-        if k == 2:
-            gather(a, way, 2, opp, way).wait_recv()
-        else:
-            gather(a, way, k, came[way], k if way == 0 else 1 - k).wait_recv()
+        gather(a, way, k).wait_recv()
 
     def pass_on(a):
         for way in range(2):
             gather_in(a, way, 0)
-            gather(a, way, 2, came[way], way).start()
+            gather(a, way, 2).start()
 
     nt = 256
 
     def rows_of(slot):
-        return pl.ds(pl.multiple_of(slot * rows, rows), rows)
+        return pl.ds(slot * rows, rows)
 
     def turned_cot(e, slot):
         cott[e * hd : (e + 1) * hd, rows_of(slot)] = cot[e, slot].T
@@ -158,11 +161,17 @@
 
     def x_first(way):
         return remote(
-            part.at[opp, pl.ds(way * half, half), :], xhalf.at[way], xs_s.at[way], xs_r.at[way], to[way]
+            part.at[OPP, pl.ds(way * half, half), :], xhalf.at[way], xs_s.at[way], xs_r.at[way], to[way]
         )
 
-    def x_second(way):
-        return remote(part.at[(nxt, prv)[way]], xfull.at[way], xs_s.at[2 + way], xs_r.at[2 + way], to[way])
+    def x_second(way, direct):
+        at = pl.ds((1 - way if direct else way) * half, half)
+        n = (4 if direct else 2) + way
+        return remote(part.at[(NXT, PRV)[way], at, :], xfull.at[way, at, :], xs_s.at[n], xs_r.at[n], to[way])
+
+    def x_direct():
+        for way in range(2):
+            x_second(way, True).start()
 
     def x_start():
         for way in range(2):
@@ -171,20 +180,21 @@
     def x_forward():
         for way in range(2):
             x_first(way).wait_recv()
-            slot = (nxt, prv)[way]
+            slot = (NXT, PRV)[way]
             for i in range(half // 16):
                 at = pl.ds(way * half + i * 16, 16)
                 got = xhalf[way, pl.ds(i * 16, 16), :].astype(F32)
                 part[slot, at, :] = (part[slot, at, :].astype(F32) + got).astype(BF16)
-            x_second(way).start()
+            x_second(way, False).start()
 
     def x_finish():
         for way in range(2):
-            x_second(way).wait_recv()
+            x_second(way, True).wait_recv()
+            x_second(way, False).wait_recv()
 
         def one(i, _):
             at = pl.ds(pl.multiple_of(i * 16, 16), 16)
-            total = part[x, at, :].astype(F32) + xfull[0, at, :].astype(F32) + xfull[1, at, :].astype(F32)
+            total = part[OWN, at, :].astype(F32) + xfull[0, at, :].astype(F32) + xfull[1, at, :].astype(F32)
             ig_ref[at, :] = total.astype(BF16)
             return 0
 
@@ -198,14 +208,29 @@
 
     left, right, outs = (cott, tokt, tokt), (hid, gb, ub), (dg_ref, gg_ref, ug_ref)
 
-    def weight_sums(k, e):
+    early = 2 * rows
+
+    def tiles(e):
         for i in range(e * hz // zt, (e + 1) * hz // zt):
-            lines = pl.ds(i * zt * zw, zt * zw)
             for j in range(ff // nt):
-                cols = pl.ds(j * nt, nt)
+                yield i, pl.ds(i * zt * zw, zt * zw), pl.ds(j * nt, nt), j == ff // nt - 1
+
+    def first_sums(k, e):
+        for i, lines, cols, _ in tiles(e):
+            acc = jnp.dot(left[k][lines, :early], right[k][:early, cols], preferred_element_type=F32)
+            prod[k, i * zt : (i + 1) * zt, :, :, :, cols] = acc.astype(BF16).reshape(zt, NY, 2, 32, nt)
+
+    def weight_sums(k, e, begun):
+        for i, lines, cols, last in tiles(e):
+            at = (k, slice(i * zt, (i + 1) * zt), slice(None), slice(None), slice(None), cols)
+            if begun:
+                acc = jnp.dot(left[k][lines, early:], right[k][early:, cols], preferred_element_type=F32)
+                acc += prod[at].reshape(zt * zw, nt).astype(F32)
+            else:
                 acc = jnp.dot(left[k][lines, :], right[k][:, cols], preferred_element_type=F32)
-                prod[k, i * zt : (i + 1) * zt, :, :, :, cols] = acc.astype(BF16).reshape(zt, NY, 2, 32, nt)
-            pair(k, i).start()
+            prod[at] = acc.astype(BF16).reshape(zt, NY, 2, 32, nt)
+            if last:
+                pair(k, i).start()
 
     def pair_sum(k, e):
         for i in range(e * hz // zt, (e + 1) * hz // zt):
@@ -245,6 +270,11 @@
         src = sa[k].at[place(along_z(owner * sgn)), y]
         return remote(src, za[k].at[m], *sems(k, e, 0, 3 + m), dev_z(target * sgn))
 
+    def a_c(k, e, way, step):
+        m = step if way == 0 else lz[0] + step
+        src = sa[k].at[place(along_z((lz[way] - step) * go(way))), y]
+        return remote(src, za[k].at[m], *sems(k, e, 0, 3 + m), dev_z(go(way)))
+
     def b_z(k, e, way, step):
         m = step if way == 0 else lz[0] + step
         src = sb[k].at[place(along_z((lz[way] - step) * go(way)))]
@@ -261,6 +291,32 @@
         for got in arrived:
             v += got.astype(F32)
         return v
+
+    def a_chain(k, e, n):
+        def run(rest_of):
+            def go_on():
+                for way in range(2):
+                    if n >= lz[way] or (lz[way] - n) % 2 != rest_of:
+                        continue
+                    if n > 0:
+                        a_c(k, e, way, n - 1).wait_recv()
+                        at = (place(along_z((lz[way] - n) * go(way))), y)
+                        got = za[k][n - 1 if way == 0 else lz[0] + n - 1]
+                        sa[k][at] = added(sa[k], at, [got]).astype(BF16)
+                    a_c(k, e, way, n).start()
+
+            return go_on
+
+        def end():
+            a_c(k, e, 0, 3).wait_recv()
+            a_c(k, e, 1, 2).wait_recv()
+            v = added(sa[k], (place(z), y), [za[k][3], za[k][6]])
+            outs[k][:, : WIDTH_A[k]] = v * scale
+
+        if n < lz[0]:
+            on_parity(e, run(0), run(1))
+        else:
+            on_parity(e, end)
 
     def a_stage(k, e, n):
         names = "abcdefg"
@@ -279,6 +335,9 @@
             a_y(k, e, 1, 0).wait_recv()
             for i in range(e * hz, (e + 1) * hz):
                 sa[k][i, y] = added(sa[k], (i, y), [ya[k][1, i], ya[k][2, i]]).astype(BF16)
+            if k in CHAINED:
+                a_chain(k, e, 0)
+                return
 
             def yes():
                 for name in "af":
@@ -289,6 +348,8 @@
                     a_z(k, e, name).start()
 
             on_parity(e, yes, no)
+        elif k in CHAINED:
+            a_chain(k, e, n - 2)
         elif n == 3:
 
             def relay(one, two, step, out):
@@ -360,7 +421,7 @@
     gather_out(0)
     loads[1].wait()
     loads[2].wait()
-    forward(x)
+    forward(OWN)
     turn_weights()
     pass_on(0)
     for load in loads[3 : 3 + nz]:
@@ -368,134 +429,147 @@
     gather_out(1)
     for load in loads[3 + nz :]:
         load.wait()
-    hid_part(x)
-    turned_cot(0, x)
-    backward(x)
-    turned_cot(1, x)
-    input_part(x)
+    hid_part(OWN)
+    turned_cot(0, OWN)
+    backward(OWN)
+    turned_cot(1, OWN)
+    input_part(OWN)
     gather_in(0, 0, 1)
-    forward(prv)
+    forward(PRV)
     gather_in(0, 1, 1)
-    forward(nxt)
+    forward(NXT)
     gather_in(0, 0, 2)
     gather_in(0, 1, 2)
-    forward(opp)
+    forward(OPP)
     pass_on(1)
     gather_out(2)
     gather_in(1, 0, 1)
-    hid_part(prv)
-    turned_cot(0, prv)
+    hid_part(PRV)
+    turned_cot(0, PRV)
     gather_in(1, 1, 1)
-    hid_part(nxt)
-    turned_cot(0, nxt)
+    hid_part(NXT)
+    turned_cot(0, NXT)
+    first_sums(0, 0)
     gather_in(1, 0, 2)
     gather_in(1, 1, 2)
-    turned_cot(0, opp)
-    weight_sums(0, 0)
+    turned_cot(0, OPP)
+    weight_sums(0, 0, True)
     pass_on(2)
     pair_sum(0, 0)
+    stage(0, 0, 1, 0)
     stage(0, 0, 0, 0)
-    stage(0, 0, 1, 0)
     gather_in(2, 0, 1)
     gather_in(2, 1, 1)
-    backward(nxt)
-    turned_cot(1, nxt)
-    backward(prv)
-    turned_cot(1, prv)
-    hid_part(opp)
+    hid_part(OPP)
+    backward(NXT)
+    turned_cot(1, NXT)
+    first_sums(1, 0)
+    first_sums(0, 1)
+    backward(PRV)
+    turned_cot(1, PRV)
     stage(0, 0, 1, 1)
+    first_sums(1, 1)
+    stage(0, 0, 0, 1)
     gather_in(2, 0, 2)
     gather_in(2, 1, 2)
-    turned_cot(1, opp)
-    weight_sums(0, 1)
-    backward(opp)
-    stage(0, 0, 0, 1)
-    weight_sums(1, 0)
+    turned_cot(1, OPP)
+    weight_sums(0, 1, True)
+    backward(OPP)
+    weight_sums(1, 0, True)
     pair_sum(0, 1)
+    stage(0, 1, 1, 0)
     stage(0, 1, 0, 0)
-    stage(0, 1, 1, 0)
-    weight_sums(1, 1)
+    weight_sums(1, 1, True)
     pair_sum(1, 0)
     stage(1, 0, 1, 0)
     stage(1, 0, 0, 0)
-    stage(0, 0, 1, 2)
-    weight_sums(2, 0)
+    weight_sums(2, 0, False)
     pair_sum(1, 1)
-    stage(1, 1, 0, 0)
     stage(1, 1, 1, 0)
-    weight_sums(2, 1)
-    stage(0, 0, 0, 2)
     stage(0, 1, 1, 1)
     pair_sum(2, 0)
-    input_part(opp)
+    stage(0, 0, 0, 2)
     stage(2, 0, 1, 0)
     stage(2, 0, 0, 0)
+    weight_sums(2, 1, False)
+    stage(1, 1, 0, 0)
+    stage(1, 0, 1, 1)
+    input_part(NXT)
     stage(1, 1, 1, 1)
+    input_part(OPP)
     pair_sum(2, 1)
-    stage(1, 0, 1, 1)
+    stage(0, 0, 0, 3)
+    stage(0, 0, 1, 2)
+    x_start()
+    stage(2, 1, 1, 0)
+    stage(1, 0, 0, 1)
+    stage(0, 1, 0, 1)
+    stage(2, 0, 1, 1)
+    stage(2, 1, 0, 0)
+    stage(1, 1, 1, 2)
+    input_part(PRV)
+    stage(0, 1, 1, 2)
+    stage(1, 1, 0, 1)
+    stage(2, 1, 1, 1)
+    x_direct()
     stage(0, 0, 1, 3)
-    x_start()
-    stage(1, 1, 0, 1)
-    stage(2, 1, 1, 0)
-    stage(2, 0, 1, 1)
-    stage(0, 1, 0, 1)
-    stage(0, 1, 1, 2)
-    input_part(prv)
-    stage(2, 1, 0, 0)
-    stage(1, 0, 0, 1)
-    input_part(nxt)
     stage(1, 0, 1, 2)
-    stage(0, 0, 0, 3)
-    stage(1, 1, 1, 2)
-    stage(2, 1, 1, 1)
     stage(2, 0, 1, 2)
+    stage(0, 0, 0, 4)
+    stage(1, 1, 1, 3)
+    stage(0, 1, 0, 2)
+    stage(2, 1, 1, 2)
+    stage(1, 0, 0, 2)
     stage(2, 0, 0, 1)
     stage(1, 1, 0, 2)
+    stage(1, 0, 1, 3)
+    stage(2, 1, 0, 1)
     stage(0, 1, 1, 3)
-    stage(1, 0, 1, 3)
-    stage(0, 1, 0, 2)
+    stage(2, 0, 1, 3)
+    stage(0, 0, 1, 4)
+    stage(2, 0, 0, 2)
+    stage(1, 1, 1, 4)
+    stage(1, 1, 0, 3)
     x_forward()
-    stage(2, 1, 1, 2)
-    stage(2, 1, 0, 1)
-    stage(1, 1, 1, 3)
-    stage(2, 0, 1, 3)
-    stage(1, 0, 0, 2)
-    stage(2, 0, 0, 2)
-    stage(1, 0, 1, 4)
+    stage(1, 0, 0, 3)
+    stage(0, 1, 0, 3)
     stage(2, 1, 1, 3)
     stage(2, 1, 0, 2)
-    stage(0, 1, 0, 3)
+    stage(1, 0, 0, 4)
+    stage(1, 0, 1, 4)
+    stage(1, 1, 0, 4)
+    stage(0, 1, 0, 4)
+    stage(0, 0, 0, 5)
+    stage(2, 0, 1, 4)
+    stage(0, 1, 1, 4)
+    stage(2, 0, 0, 3)
+    stage(1, 1, 0, 5)
+    stage(0, 1, 0, 5)
     stage(2, 1, 1, 4)
-    stage(0, 1, 1, 4)
-    stage(1, 0, 1, 5)
-    stage(2, 0, 0, 3)
-    stage(1, 1, 1, 4)
-    stage(1, 1, 0, 3)
-    stage(0, 0, 1, 4)
-    stage(1, 0, 0, 3)
-    stage(2, 0, 1, 4)
-    stage(2, 1, 0, 3)
-    stage(2, 1, 1, 5)
-    x_finish()
-    stage(0, 0, 0, 4)
-    stage(2, 0, 0, 4)
-    stage(2, 0, 1, 5)
     stage(0, 0, 1, 5)
     stage(1, 1, 1, 5)
-    stage(1, 1, 0, 4)
-    stage(1, 0, 0, 4)
+    stage(2, 1, 0, 3)
+    stage(1, 0, 0, 5)
+    x_finish()
+    stage(0, 1, 0, 6)
     stage(0, 1, 1, 5)
-    stage(0, 1, 0, 4)
+    stage(1, 0, 0, 6)
+    stage(2, 0, 1, 5)
+    stage(2, 0, 0, 4)
+    stage(1, 0, 1, 5)
+    stage(2, 1, 1, 5)
+    stage(1, 1, 0, 6)
+    stage(0, 0, 0, 6)
     stage(2, 1, 0, 4)
 
     for a in range(3):
         for way in range(2):
-            for k in range(2):
-                gather(a, way, k, x, k if way == 0 else 1 - k).wait_send()
-            gather(a, way, 2, came[way], way).wait_send()
+            for k in range(3):
+                gather(a, way, k).wait_send()
     for way in range(2):
         x_first(way).wait_send()
-        x_second(way).wait_send()
+        x_second(way, True).wait_send()
+        x_second(way, False).wait_send()
     for k in range(3):
         for i in range(nz // zt):
             pair(k, i).wait_send()
@@ -504,10 +578,12 @@
                 a_y(k, e, way, step).wait_send()
 
     def sent(k, e, names, steps, direct):
-        for name in names:
+        for name in () if k in CHAINED else names:
             a_z(k, e, name).wait_send()
         for way, step in steps:
             b_z(k, e, way, step).wait_send()
+            if k in CHAINED:
+                a_c(k, e, way, step).wait_send()
         for m in direct:
             b_y(k, e, m).wait_send()
 
@@ -585,8 +661,8 @@
                 dma((3, 2, 3)),
                 dma((3, nz // 2)),
                 dma((3, nz // 2)),
-                dma((4,)),
-                dma((4,)),
+                dma((6,)),
+                dma((6,)),
                 dma((12, 10)),
                 dma((12, 10)),
             ],

time: 83.1 us -> 86.1 us (1.036)
  Pallas kernels: 82.2 us -> 85.2 us
    pallas_call x1, Pallas kernels: 81.3 us -> 84.3 us  [on_device(): pl.pallas_call(functools.partial(body, nz, scale), out_shape=tuple((pltpu...]
where the time goes in v5:
time: 86.1 us; the launch traced here: 86 us
  Pallas kernels  85.2 us (99%)
    pallas_call x1, Pallas kernels, on_device(): pl.pallas_call(functools.partial(body, nz, scale), out_shape=tuple((pltpu...  84.3 us

profile of v5, /device:TPU:32, one launch (start us, length us, event | category | flops | bytes accessed | tf_op | source)
XLA Modules:
  0.0 86.0 jit_solution(10069805532230875173)
XLA Ops:
  0.6 84.3 %shard_map.84 = (bf16[128,2048]{1,0:T(8,128)(2,1)S(1)}, f32[32,768]{1,0:T(8,128)S(1)}, f32[32,768]{1,0:T(8,128)S(1)}, f32[32,768]{1,0:T(8,128)S(1)}) custom-call(bf16[128,2048]{1,0:T(8,128)(2,1)} %tok_hbm.1, bf16[128,2048]{1,0:T(8,128)(2,1)} %cot_hbm.1, bf16[2048,768]{1,0:T(8,128)(2,1)} %gw_hbm.1, bf16[2048,768]{1,0:T(8,128)(2,1)} %uw_hbm.1, ...), custom_call_target="tpu_custom_call" | custom-call | tf_op jit(solution)/shard_map/pallas_call | solution.py:627
  84.9 0.9 %shard_map.85 = (bf16[128,2048]{1,0:T(8,128)(2,1)}, f32[32,768]{1,0:T(8,128)}, f32[32,768]{1,0:T(8,128)}, f32[32,768]{1,0:T(8,128)}) custom-call(bf16[128,2048]{1,0:T(8,128)(2,1)S(1)} %get-tuple-element.8.refs_0_, f32[32,768]{1,0:T(8,128)S(1)} %get-tuple-element.9.refs_1_, f32[32,768]{1,0:T(8,128)S(1)} %get-tuple-element.10.refs_2_, ...), custom_call_target="tpu_custom_call" | custom-call | tf_op jit(solution)/shard_map/pallas_call | solution.py:673

commit v6 on v5

--- a/solution.py
+++ b/solution.py
@@ -12,7 +12,7 @@
 BF16 = jnp.bfloat16
 NY = 4
 WIDTH_A = (384, 384, 512)
-CHAINED = (0, 1)
+CHAINED = ()
 OWN, NXT, PRV, OPP = range(4)
 
 
@@ -456,110 +456,102 @@
     weight_sums(0, 0, True)
     pass_on(2)
     pair_sum(0, 0)
+    stage(0, 0, 0, 0)
     stage(0, 0, 1, 0)
-    stage(0, 0, 0, 0)
     gather_in(2, 0, 1)
     gather_in(2, 1, 1)
-    hid_part(OPP)
     backward(NXT)
     turned_cot(1, NXT)
+    backward(PRV)
+    turned_cot(1, PRV)
+    first_sums(1, 1)
     first_sums(1, 0)
     first_sums(0, 1)
-    backward(PRV)
-    turned_cot(1, PRV)
     stage(0, 0, 1, 1)
-    first_sums(1, 1)
-    stage(0, 0, 0, 1)
+    hid_part(OPP)
     gather_in(2, 0, 2)
     gather_in(2, 1, 2)
     turned_cot(1, OPP)
     weight_sums(0, 1, True)
     backward(OPP)
+    stage(0, 0, 0, 1)
     weight_sums(1, 0, True)
     pair_sum(0, 1)
+    stage(0, 1, 0, 0)
     stage(0, 1, 1, 0)
-    stage(0, 1, 0, 0)
     weight_sums(1, 1, True)
+    stage(0, 0, 1, 2)
     pair_sum(1, 0)
+    stage(1, 0, 0, 0)
     stage(1, 0, 1, 0)
-    stage(1, 0, 0, 0)
     weight_sums(2, 0, False)
     pair_sum(1, 1)
     stage(1, 1, 1, 0)
     stage(0, 1, 1, 1)
     pair_sum(2, 0)
+    stage(1, 1, 0, 0)
     stage(0, 0, 0, 2)
+    weight_sums(2, 1, False)
     stage(2, 0, 1, 0)
     stage(2, 0, 0, 0)
-    weight_sums(2, 1, False)
-    stage(1, 1, 0, 0)
+    input_part(OPP)
     stage(1, 0, 1, 1)
+    stage(0, 1, 0, 1)
+    pair_sum(2, 1)
+    stage(1, 1, 1, 1)
+    stage(1, 0, 0, 1)
+    stage(2, 1, 1, 0)
+    input_part(PRV)
     input_part(NXT)
-    stage(1, 1, 1, 1)
-    input_part(OPP)
-    pair_sum(2, 1)
+    stage(0, 1, 1, 2)
+    stage(2, 1, 0, 0)
     stage(0, 0, 0, 3)
-    stage(0, 0, 1, 2)
     x_start()
-    stage(2, 1, 1, 0)
-    stage(1, 0, 0, 1)
-    stage(0, 1, 0, 1)
     stage(2, 0, 1, 1)
-    stage(2, 1, 0, 0)
-    stage(1, 1, 1, 2)
-    input_part(PRV)
-    stage(0, 1, 1, 2)
+    stage(1, 0, 1, 2)
     stage(1, 1, 0, 1)
     stage(2, 1, 1, 1)
+    stage(0, 1, 0, 2)
+    stage(0, 0, 1, 3)
+    stage(2, 0, 0, 1)
+    stage(1, 1, 1, 2)
+    stage(2, 0, 1, 2)
+    stage(2, 1, 1, 2)
+    stage(1, 0, 1, 3)
     x_direct()
-    stage(0, 0, 1, 3)
-    stage(1, 0, 1, 2)
-    stage(2, 0, 1, 2)
     stage(0, 0, 0, 4)
+    stage(0, 1, 1, 3)
+    stage(2, 1, 0, 1)
+    stage(1, 1, 0, 2)
+    stage(2, 0, 0, 2)
+    stage(0, 0, 1, 4)
+    stage(1, 0, 0, 2)
+    stage(2, 1, 1, 3)
+    stage(0, 1, 1, 4)
     stage(1, 1, 1, 3)
-    stage(0, 1, 0, 2)
-    stage(2, 1, 1, 2)
-    stage(1, 0, 0, 2)
-    stage(2, 0, 0, 1)
-    stage(1, 1, 0, 2)
-    stage(1, 0, 1, 3)
-    stage(2, 1, 0, 1)
-    stage(0, 1, 1, 3)
+    stage(2, 1, 0, 2)
     stage(2, 0, 1, 3)
-    stage(0, 0, 1, 4)
-    stage(2, 0, 0, 2)
+    x_forward()
+    stage(2, 1, 1, 4)
+    stage(2, 0, 0, 3)
+    stage(1, 1, 0, 3)
+    stage(0, 1, 0, 3)
+    stage(0, 1, 1, 5)
     stage(1, 1, 1, 4)
-    stage(1, 1, 0, 3)
-    x_forward()
+    stage(1, 0, 1, 4)
     stage(1, 0, 0, 3)
-    stage(0, 1, 0, 3)
-    stage(2, 1, 1, 3)
-    stage(2, 1, 0, 2)
+    stage(2, 1, 0, 3)
+    stage(1, 1, 0, 4)
+    stage(2, 0, 1, 4)
+    x_finish()
     stage(1, 0, 0, 4)
-    stage(1, 0, 1, 4)
-    stage(1, 1, 0, 4)
     stage(0, 1, 0, 4)
-    stage(0, 0, 0, 5)
-    stage(2, 0, 1, 4)
-    stage(0, 1, 1, 4)
-    stage(2, 0, 0, 3)
-    stage(1, 1, 0, 5)
-    stage(0, 1, 0, 5)
-    stage(2, 1, 1, 4)
-    stage(0, 0, 1, 5)
-    stage(1, 1, 1, 5)
-    stage(2, 1, 0, 3)
-    stage(1, 0, 0, 5)
-    x_finish()
-    stage(0, 1, 0, 6)
-    stage(0, 1, 1, 5)
-    stage(1, 0, 0, 6)
-    stage(2, 0, 1, 5)
     stage(2, 0, 0, 4)
     stage(1, 0, 1, 5)
+    stage(2, 0, 1, 5)
+    stage(1, 1, 1, 5)
+    stage(0, 0, 1, 5)
     stage(2, 1, 1, 5)
-    stage(1, 1, 0, 6)
-    stage(0, 0, 0, 6)
     stage(2, 1, 0, 4)
 
     for a in range(3):

time: 86.1 us -> 84.2 us (0.978)
  Pallas kernels: 85.2 us -> 83 us
    pallas_call x1, Pallas kernels: 84.3 us -> 82.1 us  [on_device(): pl.pallas_call(functools.partial(body, nz, scale), out_shape=tuple((pltpu...]
where the time goes in v6:
time: 84.2 us; the launch traced here: 83.8 us
  Pallas kernels  83 us (99%)
    pallas_call x1, Pallas kernels, on_device(): pl.pallas_call(functools.partial(body, nz, scale), out_shape=tuple((pltpu...  82.1 us

profile of v6, /device:TPU:32, one launch (start us, length us, event | category | flops | bytes accessed | tf_op | source)
XLA Modules:
  0.0 83.8 jit_solution(6086012417557258700)
XLA Ops:
  0.6 82.1 %shard_map.84 = (bf16[128,2048]{1,0:T(8,128)(2,1)S(1)}, f32[32,768]{1,0:T(8,128)S(1)}, f32[32,768]{1,0:T(8,128)S(1)}, f32[32,768]{1,0:T(8,128)S(1)}) custom-call(bf16[128,2048]{1,0:T(8,128)(2,1)} %tok_hbm.1, bf16[128,2048]{1,0:T(8,128)(2,1)} %cot_hbm.1, bf16[2048,768]{1,0:T(8,128)(2,1)} %gw_hbm.1, bf16[2048,768]{1,0:T(8,128)(2,1)} %uw_hbm.1, ...), custom_call_target="tpu_custom_call" | custom-call | tf_op jit(solution)/shard_map/pallas_call | solution.py:619
  82.8 0.9 %shard_map.85 = (bf16[128,2048]{1,0:T(8,128)(2,1)}, f32[32,768]{1,0:T(8,128)}, f32[32,768]{1,0:T(8,128)}, f32[32,768]{1,0:T(8,128)}) custom-call(bf16[128,2048]{1,0:T(8,128)(2,1)S(1)} %get-tuple-element.8.refs_0_, f32[32,768]{1,0:T(8,128)S(1)} %get-tuple-element.9.refs_1_, f32[32,768]{1,0:T(8,128)S(1)} %get-tuple-element.10.refs_2_, ...), custom_call_target="tpu_custom_call" | custom-call | tf_op jit(solution)/shard_map/pallas_call | solution.py:665

commit v7 on v5

--- a/solution.py
+++ b/solution.py
@@ -11,8 +11,8 @@
 F32 = jnp.float32
 BF16 = jnp.bfloat16
 NY = 4
-WIDTH_A = (384, 384, 512)
-CHAINED = (0, 1)
+WIDTH_A = (384, 384, 640)
+CHAINED = ()
 OWN, NXT, PRV, OPP = range(4)
 
 
@@ -456,110 +456,102 @@
     weight_sums(0, 0, True)
     pass_on(2)
     pair_sum(0, 0)
+    stage(0, 0, 0, 0)
     stage(0, 0, 1, 0)
-    stage(0, 0, 0, 0)
     gather_in(2, 0, 1)
     gather_in(2, 1, 1)
-    hid_part(OPP)
     backward(NXT)
     turned_cot(1, NXT)
-    first_sums(1, 0)
-    first_sums(0, 1)
     backward(PRV)
     turned_cot(1, PRV)
+    first_sums(0, 1)
+    first_sums(1, 0)
+    first_sums(1, 1)
+    hid_part(OPP)
     stage(0, 0, 1, 1)
-    first_sums(1, 1)
-    stage(0, 0, 0, 1)
     gather_in(2, 0, 2)
     gather_in(2, 1, 2)
     turned_cot(1, OPP)
     weight_sums(0, 1, True)
     backward(OPP)
+    stage(0, 0, 0, 1)
     weight_sums(1, 0, True)
     pair_sum(0, 1)
+    stage(0, 1, 0, 0)
     stage(0, 1, 1, 0)
-    stage(0, 1, 0, 0)
     weight_sums(1, 1, True)
     pair_sum(1, 0)
     stage(1, 0, 1, 0)
     stage(1, 0, 0, 0)
+    stage(0, 0, 1, 2)
     weight_sums(2, 0, False)
     pair_sum(1, 1)
+    stage(1, 1, 0, 0)
     stage(1, 1, 1, 0)
+    weight_sums(2, 1, False)
+    stage(0, 0, 0, 2)
     stage(0, 1, 1, 1)
     pair_sum(2, 0)
-    stage(0, 0, 0, 2)
+    input_part(OPP)
     stage(2, 0, 1, 0)
     stage(2, 0, 0, 0)
-    weight_sums(2, 1, False)
-    stage(1, 1, 0, 0)
+    stage(1, 1, 1, 1)
+    pair_sum(2, 1)
     stage(1, 0, 1, 1)
+    stage(0, 0, 1, 3)
+    x_start()
+    stage(1, 1, 0, 1)
+    stage(2, 1, 1, 0)
+    stage(2, 0, 1, 1)
+    stage(0, 1, 0, 1)
+    stage(0, 1, 1, 2)
+    input_part(PRV)
+    stage(2, 1, 0, 0)
+    stage(1, 0, 0, 1)
     input_part(NXT)
-    stage(1, 1, 1, 1)
-    input_part(OPP)
-    pair_sum(2, 1)
+    x_direct()
+    stage(1, 0, 1, 2)
     stage(0, 0, 0, 3)
-    stage(0, 0, 1, 2)
-    x_start()
-    stage(2, 1, 1, 0)
-    stage(1, 0, 0, 1)
-    stage(0, 1, 0, 1)
-    stage(2, 0, 1, 1)
-    stage(2, 1, 0, 0)
     stage(1, 1, 1, 2)
-    input_part(PRV)
-    stage(0, 1, 1, 2)
-    stage(1, 1, 0, 1)
     stage(2, 1, 1, 1)
-    x_direct()
-    stage(0, 0, 1, 3)
-    stage(1, 0, 1, 2)
     stage(2, 0, 1, 2)
-    stage(0, 0, 0, 4)
-    stage(1, 1, 1, 3)
-    stage(0, 1, 0, 2)
-    stage(2, 1, 1, 2)
-    stage(1, 0, 0, 2)
     stage(2, 0, 0, 1)
     stage(1, 1, 0, 2)
+    stage(0, 1, 1, 3)
     stage(1, 0, 1, 3)
+    stage(0, 1, 0, 2)
+    x_forward()
+    stage(2, 1, 1, 2)
     stage(2, 1, 0, 1)
-    stage(0, 1, 1, 3)
+    stage(1, 1, 1, 3)
     stage(2, 0, 1, 3)
-    stage(0, 0, 1, 4)
+    stage(1, 0, 0, 2)
     stage(2, 0, 0, 2)
+    stage(1, 0, 1, 4)
+    stage(2, 1, 1, 3)
+    stage(2, 1, 0, 2)
+    stage(0, 1, 0, 3)
+    stage(2, 1, 1, 4)
+    stage(0, 1, 1, 4)
+    stage(1, 0, 1, 5)
+    stage(2, 0, 0, 3)
     stage(1, 1, 1, 4)
     stage(1, 1, 0, 3)
-    x_forward()
+    stage(0, 0, 1, 4)
     stage(1, 0, 0, 3)
-    stage(0, 1, 0, 3)
-    stage(2, 1, 1, 3)
-    stage(2, 1, 0, 2)
-    stage(1, 0, 0, 4)
-    stage(1, 0, 1, 4)
-    stage(1, 1, 0, 4)
-    stage(0, 1, 0, 4)
-    stage(0, 0, 0, 5)
     stage(2, 0, 1, 4)
-    stage(0, 1, 1, 4)
-    stage(2, 0, 0, 3)
-    stage(1, 1, 0, 5)
-    stage(0, 1, 0, 5)
-    stage(2, 1, 1, 4)
+    stage(2, 1, 0, 3)
+    stage(2, 1, 1, 5)
+    x_finish()
+    stage(0, 0, 0, 4)
+    stage(2, 0, 0, 4)
+    stage(2, 0, 1, 5)
     stage(0, 0, 1, 5)
     stage(1, 1, 1, 5)
-    stage(2, 1, 0, 3)
-    stage(1, 0, 0, 5)
-    x_finish()
-    stage(0, 1, 0, 6)
+    stage(1, 1, 0, 4)
+    stage(1, 0, 0, 4)
     stage(0, 1, 1, 5)
-    stage(1, 0, 0, 6)
-    stage(2, 0, 1, 5)
-    stage(2, 0, 0, 4)
-    stage(1, 0, 1, 5)
-    stage(2, 1, 1, 5)
-    stage(1, 1, 0, 6)
-    stage(0, 0, 0, 6)
+    stage(0, 1, 0, 4)
     stage(2, 1, 0, 4)
 
     for a in range(3):

time: 86.1 us -> 83.3 us (0.967)
  Pallas kernels: 85.2 us -> 82.4 us
    pallas_call x1, Pallas kernels: 84.3 us -> 81.5 us  [on_device(): pl.pallas_call(functools.partial(body, nz, scale), out_shape=tuple((pltpu...]
where the time goes in v7:
time: 83.3 us; the launch traced here: 83.2 us
  Pallas kernels  82.4 us (99%)
    pallas_call x1, Pallas kernels, on_device(): pl.pallas_call(functools.partial(body, nz, scale), out_shape=tuple((pltpu...  81.5 us

profile of v7, /device:TPU:32, one launch (start us, length us, event | category | flops | bytes accessed | tf_op | source)
XLA Modules:
  0.0 83.2 jit_solution(551313266005097735)
XLA Ops:
  0.6 81.5 %shard_map.84 = (bf16[128,2048]{1,0:T(8,128)(2,1)S(1)}, f32[32,768]{1,0:T(8,128)S(1)}, f32[32,768]{1,0:T(8,128)S(1)}, f32[32,768]{1,0:T(8,128)S(1)}) custom-call(bf16[128,2048]{1,0:T(8,128)(2,1)} %tok_hbm.1, bf16[128,2048]{1,0:T(8,128)(2,1)} %cot_hbm.1, bf16[2048,768]{1,0:T(8,128)(2,1)} %gw_hbm.1, bf16[2048,768]{1,0:T(8,128)(2,1)} %uw_hbm.1, ...), custom_call_target="tpu_custom_call" | custom-call | tf_op jit(solution)/shard_map/pallas_call | solution.py:619
  82.1 0.9 %shard_map.85 = (bf16[128,2048]{1,0:T(8,128)(2,1)}, f32[32,768]{1,0:T(8,128)}, f32[32,768]{1,0:T(8,128)}, f32[32,768]{1,0:T(8,128)}) custom-call(bf16[128,2048]{1,0:T(8,128)(2,1)S(1)} %get-tuple-element.8.refs_0_, f32[32,768]{1,0:T(8,128)S(1)} %get-tuple-element.9.refs_1_, f32[32,768]{1,0:T(8,128)S(1)} %get-tuple-element.10.refs_2_, ...), custom_call_target="tpu_custom_call" | custom-call | tf_op jit(solution)/shard_map/pallas_call | solution.py:665
